TPU v7x, 256 devices: a whole 4x4x8 slice. The times are simulated.
256 devices in a mesh: ep: 64 (over z, x, core), tp: 4 (over y).
Axes of the slice: x: 4, y: 4, z: 8, core: 2. Of those that a mesh axis runs over, the one named last changes fastest.
Arguments:
- mixer_input: bfloat16 [32768, 2048], P('ep'), may hold values from -6 to 6
- mixer_gain: float32 [2048], replicated, may hold values from 0.1 to 1.9
- query_weight: bfloat16 [2048, 1024], P(None, 'tp'), may hold values from -0.125 to 0.125
- key_weight: bfloat16 [2048, 1024], P(None, 'tp'), may hold values from -0.125 to 0.125
- value_weight: bfloat16 [2048, 1024], P(None, 'tp'), may hold values from -0.125 to 0.125
- gate_weight: bfloat16 [2048, 1024], P(None, 'tp'), may hold values from -0.125 to 0.125
- head_gain: float32 [1024], P('tp'), may hold values from 0.1 to 1.9
- output_weight: bfloat16 [1024, 2048], P('tp'), may hold values from -0.1875 to 0.1875
- log_decay: float32 [32768, 8], P('ep', 'tp'), may hold values from -1 to 0, as said below
- expert_input: bfloat16 [32768, 2048], P(('ep', 'tp')), may hold values from -6 to 6
- expert_gain: float32 [2048], replicated, may hold values from 0.1 to 1.9
- routes: int32 [32768, 2], P(('ep', 'tp')), may hold values from 0 to 63, all different within a row; in each aligned block of 128 rows (0 to 127, 128 to 255, ...) at most 6 rows name the same one
- route_weight: float32 [32768, 2], P(('ep', 'tp')), may hold values from 0.1 to 1
- expert_gate: bfloat16 [64, 2048, 1024], P('ep', None, 'tp'), may hold values from -0.125 to 0.125
- expert_up: bfloat16 [64, 2048, 1024], P('ep', None, 'tp'), may hold values from -0.125 to 0.125
- expert_down: bfloat16 [64, 1024, 2048], P('ep', 'tp'), may hold values from -0.1875 to 0.1875
Outputs:
- mixer_output: bfloat16 [32768, 2048], P(('ep', 'tp'))
- expert_output: bfloat16 [32768, 2048], P(('ep', 'tp'))
Inputs may be any that keep to these rules, and one draw needn't show every extreme that they name: `routes`: each row names 2 different experts. Among the rows of one device no expert is named more than 6 times, and in every draw the rows of some device name some expert exactly 6 times. `log_decay`: negative values.
All inputs are finite; a program needn't handle non-finite values.
Results may differ from a plain program's by a relative error of at most 0.025.
Values may be sent and summed in bfloat16 or wider, within the bound.
A program may use at most 128 MiB of HBM per device.

v0:
```python
import jax
import jax.numpy as jnp
from jax import lax
from jax.sharding import Mesh
from jax.sharding import PartitionSpec as P

BLOCK = 128
EP = ("ep_0", "ep_1", "ep_2")
EP_TP = ("ep_0", "ep_1", "ep_2", "tp")


EPS = 1e-06


def filled_with(x, identity):
    return jax.tree.map(
        lambda part, zero: jnp.zeros_like(part) + jnp.asarray(zero, part.dtype), x, identity
    )


def carried_in(x, axes, combine, identity):
    before = start = filled_with(x, identity)
    running = x
    for axis in reversed(axes):
        peers, position = (lax.axis_size(axis), lax.axis_index(axis))
        pieces = jax.tree.map(
            lambda part, kind: lax.all_gather(part.astype(kind), axis),
            running,
            (jnp.bfloat16, jnp.bfloat16),
        )
        inside, running = (start, start)
        for k in range(peers):
            passed = k < position
            running = combine(
                running, jax.tree.map(lambda part, own: part[k].astype(own.dtype), pieces, x)
            )
            inside = jax.tree.map(lambda new, old: jnp.where(passed, new, old), running, inside)
        before = combine(inside, before)
    return before


def norm_rows(values, gain):
    floats = values.astype(jnp.float32)
    scale = lax.rsqrt(jnp.mean(floats * floats, axis=-1, keepdims=True) + EPS)
    return (floats * scale * gain).astype(jnp.bfloat16)


def rotate(values, position):
    half_dim = values.shape[-1] // 2
    frequency = 10000.0 ** (-jnp.arange(half_dim, dtype=jnp.float32) / half_dim)
    angles = position.astype(jnp.float32)[:, None] * frequency[None, :]
    cosine = jnp.cos(angles)[:, None, :]
    sine_part = jnp.sin(angles)[:, None, :]
    first_half = values[..., :half_dim]
    second = values[..., half_dim:]
    return jnp.concatenate(
        [first_half * cosine - second * sine_part, first_half * sine_part + second * cosine],
        axis=-1,
    )


def chain_pair(earlier, following):
    return (earlier[0] * following[0], following[0][:, None, None] * earlier[1] + following[1])


def mixer_half(
    mixer_input,
    mixer_gain,
    query_weight,
    key_weight,
    value_weight,
    gate_weight,
    head_gain,
    output_weight,
    log_decay,
):
    row_count = mixer_input.shape[0]
    head_count = log_decay.shape[1]
    mix_width = query_weight.shape[1]
    head_dim = mix_width // head_count
    normed = norm_rows(mixer_input, mixer_gain)

    def project(weight):
        return jnp.dot(normed, weight, preferred_element_type=jnp.float32).astype(jnp.bfloat16)

    queries = project(query_weight)
    keys_raw = project(key_weight)
    values_new = project(value_weight)
    gate_raw = project(gate_weight)
    position = lax.axis_index(EP) * row_count + jnp.arange(row_count, dtype=jnp.int32)
    q_rot = rotate(
        queries.astype(jnp.float32).reshape(row_count, head_count, head_dim), position
    ).astype(jnp.bfloat16)
    k_rot = (
        rotate(keys_raw.astype(jnp.float32).reshape(row_count, head_count, head_dim), position)
        * head_dim ** (-0.5)
    ).astype(jnp.bfloat16)
    block_count = row_count // BLOCK
    q_blocks = q_rot.reshape(block_count, BLOCK, head_count, head_dim)
    k_blocks = k_rot.reshape(block_count, BLOCK, head_count, head_dim)
    v_blocks = values_new.reshape(block_count, BLOCK, head_count, head_dim)
    log_steps = log_decay.reshape(block_count, BLOCK, head_count)
    row_ids = lax.broadcasted_iota(jnp.int32, (BLOCK, BLOCK), 0)
    col_ids = lax.broadcasted_iota(jnp.int32, (BLOCK, BLOCK), 1)
    lower_mask = col_ids <= row_ids
    cumulative = jnp.einsum("ij,bjh->bhi", lower_mask.astype(jnp.float32), log_steps)
    block_total = cumulative[:, :, -1]
    differences = cumulative[:, :, :, None] - cumulative[:, :, None, :]
    decays = jnp.where(lower_mask, jnp.exp(jnp.where(lower_mask, differences, 0.0)), 0.0)
    scores = jnp.einsum("bihd,bjhd->bhij", q_blocks, k_blocks, preferred_element_type=jnp.float32)
    weights = (scores * decays).astype(jnp.bfloat16)
    inner_term = jnp.einsum(
        "bhij,bjhe->bihe", weights, v_blocks, preferred_element_type=jnp.float32
    )
    key_scale = jnp.exp(block_total[:, :, None] - cumulative)
    updates = jnp.einsum(
        "bhj,bjhd,bjhe->bhde", key_scale, k_blocks.astype(jnp.float32), v_blocks.astype(jnp.float32)
    )
    factor = jnp.exp(block_total)
    local_state = jnp.zeros((head_count, head_dim, head_dim), jnp.float32)
    for block_index in range(block_count):
        local_state = factor[block_index][:, None, None] * local_state + updates[block_index]
    entering = carried_in(
        (jnp.exp(jnp.sum(block_total, axis=0)), local_state),
        EP,
        chain_pair,
        (jnp.ones((head_count,), jnp.float32), jnp.zeros_like(local_state)),
    )
    carry_state = entering[1]
    starts = []
    for block_index in range(block_count):
        starts.append(carry_state)
        carry_state = factor[block_index][:, None, None] * carry_state + updates[block_index]
    carried = jnp.stack(starts)
    cross_term = jnp.einsum(
        "bhi,bihd,bhde->bihe", jnp.exp(cumulative), q_blocks.astype(jnp.float32), carried
    )
    retained = (inner_term + cross_term).reshape(row_count, head_count, head_dim)
    centre = jnp.mean(retained, axis=-1, keepdims=True)
    spread = jnp.mean(jnp.square(retained - centre), axis=-1, keepdims=True)
    scaled = (retained - centre) * lax.rsqrt(spread + EPS) * head_gain.reshape(head_count, head_dim)
    mixer_hidden = (
        scaled.reshape(row_count, mix_width) * jax.nn.silu(gate_raw.astype(jnp.float32))
    ).astype(jnp.bfloat16)
    return lax.psum_scatter(
        jnp.dot(mixer_hidden, output_weight, preferred_element_type=jnp.float32).astype(
            jnp.bfloat16
        ),
        "tp",
        scatter_dimension=0,
        tiled=True,
    )


def expert_half(
    expert_input, expert_gain, routes, route_weight, expert_gate, expert_up, expert_down
):
    tok_count, top_count = routes.shape
    experts = lax.axis_size(EP)
    capacity = max(2, 3 * tok_count * top_count // (2 * experts))
    width = expert_input.shape[1]
    normed = norm_rows(expert_input, expert_gain)
    flat_routes = routes.reshape(-1)
    entries = flat_routes.shape[0]
    onehot = (flat_routes[:, None] == jnp.arange(experts, dtype=jnp.int32)[None, :]).astype(
        jnp.bfloat16
    )
    before = (
        lax.broadcasted_iota(jnp.int32, (entries, entries), 1)
        < lax.broadcasted_iota(jnp.int32, (entries, entries), 0)
    ).astype(jnp.bfloat16)
    prior_count = jnp.dot(before, onehot, preferred_element_type=jnp.float32)
    slot_index = jnp.sum(prior_count * onehot.astype(jnp.float32), axis=1).astype(jnp.int32)
    target = flat_routes * capacity + slot_index
    token_ids = jnp.arange(entries, dtype=jnp.int32) // top_count
    slot_table = jnp.full((experts * capacity,), tok_count, jnp.int32).at[target].set(token_ids)
    padded = jnp.concatenate([normed, jnp.zeros((1, width), jnp.bfloat16)], axis=0)
    outgoing = jnp.take(padded, slot_table, axis=0).reshape(experts, capacity, width)
    arrived = lax.all_to_all(outgoing, EP, split_axis=0, concat_axis=0, tiled=True)
    sources = arrived.shape[0]
    flat_rows = arrived.reshape(sources * capacity, width)
    shard_piece = lax.all_gather((expert_gate[0], expert_up[0]), "tp", axis=1, tiled=True)
    gate_part = jnp.dot(flat_rows, shard_piece[0], preferred_element_type=jnp.float32)
    up_part = jnp.dot(flat_rows, shard_piece[1], preferred_element_type=jnp.float32)
    hidden = (jax.nn.silu(gate_part) * up_part).astype(jnp.bfloat16)
    reduced = jnp.dot(
        hidden,
        lax.all_gather(expert_down[0], "tp", axis=0, tiled=True),
        preferred_element_type=jnp.float32,
    )
    results = reduced.astype(jnp.bfloat16).reshape(sources, capacity, width)
    returned = lax.all_to_all(results, EP, split_axis=0, concat_axis=0, tiled=True)
    picked = jnp.take(returned.reshape(experts * capacity, width), target, axis=0)
    picked = picked.astype(jnp.float32).reshape(tok_count, top_count, width)
    norm_weight = route_weight / jnp.sum(route_weight, axis=1, keepdims=True)
    return jnp.sum(picked * norm_weight[:, :, None], axis=1).astype(jnp.bfloat16)


def on_device(
    mixer_input,
    mixer_gain,
    query_weight,
    key_weight,
    value_weight,
    gate_weight,
    head_gain,
    output_weight,
    log_decay,
    expert_input,
    expert_gain,
    routes,
    route_weight,
    expert_gate,
    expert_up,
    expert_down,
):
    mixer_output = mixer_half(
        mixer_input,
        mixer_gain,
        query_weight,
        key_weight,
        value_weight,
        gate_weight,
        head_gain,
        output_weight,
        log_decay,
    )
    expert_output = expert_half(
        expert_input, expert_gain, routes, route_weight, expert_gate, expert_up, expert_down
    )
    return (mixer_output, expert_output)


def solution(mesh):
    finer = Mesh(mesh.devices.reshape(8, 4, 2, mesh.shape["tp"]), ("ep_0", "ep_1", "ep_2", "tp"))
    placed = (
        P(EP, None),
        P(),
        P(None, "tp"),
        P(None, "tp"),
        P(None, "tp"),
        P(None, "tp"),
        P("tp"),
        P("tp", None),
        P(EP, "tp"),
        P(EP_TP, None),
        P(),
        P(EP_TP, None),
        P(EP_TP, None),
        P(EP, None, "tp"),
        P(EP, None, "tp"),
        P(EP, "tp", None),
    )
    return jax.shard_map(
        on_device,
        mesh=finer,
        in_specs=placed,
        out_specs=(P(EP_TP, None), P(EP_TP, None)),
        check_vma=False,
    )
```

profile of v0, /device:TPU:2, one launch (start us, length us, event | category | flops | bytes accessed | tf_op | source)
XLA Modules:
  0.0 269.4 jit_solution(11428957834506784839)
XLA Ops:
  11.4 3.1 %gather_fusion = bf16[384,2048]{1,0:T(8,128)(2,1)} fusion(bf16[129,2048]{1,0:T(8,128)(2,1)S(1)} %concatenate.26, s32[1024]{0:T(1024)S(1)} %pad_clamp_fusion.1), kind=kCustom, calls=%fused_computation | custom fusion | bytes 3147264 | tf_op jit(solution)/shard_map/jit(_take)/gather | solution.py:178
  14.5 2.5 gather.13
  17.2 1.6 broadcast_select_fusion
  18.8 12.0 %all-to-all-start = ((bf16[64,6,2048]{2,1,0:T(8,128)(2,1)}), bf16[64,6,2048]{2,1,0:T(8,128)(2,1)S(1)}, u32[]{:S(2)}, u32[]{:S(2)}) async-start(bf16[64,6,2048]{2,1,0:T(8,128)(2,1)} %broadcast_select_fusion), calls=%async_computation.1 | async-start | bytes 4194304 | tf_op jit(solution)/shard_map/all_to_all | solution.py:179
  31.7 2.1 fusion
  35.4 2.8 %convolution_convert_fusion.3 = bf16[512,256]{0,1:T(8,128)(2,1)S(1)} fusion(bf16[2048,256]{1,0:T(8,128)(2,1)} %param.18, bf16[512,2048]{1,0:T(8,128)(2,1)} %param.16, f32[2048]{0:T(1024)S(1)} %copy-done.25, f32[512]{0:T(512)S(1)} %add_rsqrt_fusion), kind=kOutput, calls=%fused_computation.28 | convolution fusion | flops 541196288 | bytes 3418112 | tf_op jit(solution)/shard_map/dot_general | solution.py:84
  38.4 3.5 %convolution_convert_fusion.2 = bf16[512,256]{0,1:T(8,128)(2,1)} fusion(bf16[2048,256]{1,0:T(8,128)(2,1)} %param.19, bf16[512,2048]{1,0:T(8,128)(2,1)} %param.16, f32[2048]{0:T(1024)S(1)} %copy-done.25, f32[512]{0:T(512)S(1)} %add_rsqrt_fusion), kind=kOutput, calls=%fused_computation.27 | convolution fusion | flops 541196288 | bytes 3418112 | tf_op jit(solution)/shard_map/dot_general | solution.py:84
  41.9 2.4 all-reduce.1
  44.9 7.8 %all-gather.4 = bf16[4,1,2]{2,1,0:T(2,128)(2,1)S(1)} all-gather(bf16[1,1,2]{2,1,0:T(2,128)(2,1)S(1)} %convert_bitcast_fusion), channel_id=1, replica_groups=mesh['ep_0'=8,'ep_1'=4,'ep_2'=2,'tp'=4] {'ep_1'}, dimensions={0}, use_global_device_ids=true | all-gather | bytes 20 | tf_op jit(solution)/shard_map/all_gather | solution.py:27
  53.6 1.8 convert.28
  55.9 2.3 subtract_convert_fusion
  62.4 2.6 convolution_convert_fusion.4
  69.8 1.9 all_gather.36
  75.1 16.2 %all-gather.5 = bf16[8,1,2]{2,1,0:T(2,128)(2,1)S(1)} all-gather(bf16[1,1,2]{2,1,0:T(2,128)(2,1)S(1)} %fusion.73), channel_id=1, replica_groups=mesh['ep_0'=8,'ep_1'=4,'ep_2'=2,'tp'=4] {'ep_0'}, dimensions={0}, use_global_device_ids=true | all-gather | bytes 36 | tf_op jit(solution)/shard_map/all_gather | solution.py:27
  93.5 1.8 copy.59
  96.9 1.8 copy.60
  98.6 12.1 %all_gather.37 = bf16[4,2,128,128]{3,2,1,0:T(8,128)(2,1)S(1)} all-gather(bf16[1,2,128,128]{3,2,1,0:T(8,128)(2,1)} %fusion.56), channel_id=1, replica_groups=mesh['ep_0'=8,'ep_1'=4,'ep_2'=2,'tp'=4] {'ep_1'}, dimensions={0}, use_global_device_ids=true | all-gather | bytes 327680 | tf_op jit(solution)/shard_map/all_gather | solution.py:27
  111.5 25.7 %all_gather.38 = bf16[8,2,128,128]{3,2,1,0:T(8,128)(2,1)S(1)} all-gather(bf16[1,2,128,128]{3,2,1,0:T(8,128)(2,1)S(1)} %fusion.55), channel_id=1, replica_groups=mesh['ep_0'=8,'ep_1'=4,'ep_2'=2,'tp'=4] {'ep_0'}, dimensions={0}, use_global_device_ids=true | all-gather | bytes 589824 | tf_op jit(solution)/shard_map/all_gather | solution.py:27
  140.1 2.8 %fusion.90 = (f32[4,128,2]{1,2,0:T(2,128)S(1)}, f32[4,128,2,128]{1,3,2,0:T(8,128)}) fusion(f32[4,128,2,128]{1,3,2,0:T(8,128)} %convolution_bitcast_fusion.1, bf16[4,128,2,128]{3,1,2,0:T(8,128)(2,1)S(1)} %fusion.27, f32[4,2,128]{2,1,0:T(2,128)S(1)} %copy-done.18, pred[128,128]{1,0:T(8,128)(4,1)} %iota_compare_fusion.4, bf16[4,128,2,64]{3,1,2,0:T(8,128)(2,1)} %copy.60, ...), kind=kOutput, calls=%fused_computation.178 | convolution fusion | flops 68549632 | bytes 1859584 | tf_op jit(solution)/shard_map/bhij,bjhe->bihe/dot_general | solution.py:112
  142.9 2.1 copy.71
  148.6 2.3 sub.60
  150.9 6.0 %convolution_convert_fusion = bf16[512,2048]{1,0:T(8,128)(2,1)} fusion(bf16[256,2048]{1,0:T(8,128)(2,1)S(1)} %copy-done, f32[64,8,2,128]{3,2,1,0:T(2,128)} %bitcast.151, f32[64,8,2,128]{3,2,1,0:T(2,128)} %bitcast.152, f32[64,8,2,128]{3,2,1,0:T(2,128)} %bitcast.153, bf16[2048,256]{1,0:T(8,128)(2,1)} %param.21, f32[256]{0:T(256)S(1)} %copy-done.27, ...), kind=kOutput, calls=%fused_computation.14 | convolution fusion | flops 1080426496 | bytes 7875584 | tf_op jit(solution)/shard_map/dot_general | solution.py:146
  158.4 5.8 %fusion.7 = f32[384,1024]{1,0:T(8,128)} fusion(bf16[384,2048]{1,0:T(8,128)(2,1)} %reshape.379, bf16[1,2048,1024]{2,1,0:T(8,128)(2,1)} %all-gather.10.cloned.1.call-done), kind=kOutput, calls=%fused_computation.12 | convolution fusion | flops 1610612736 | bytes 7340032 | tf_op jit(solution)/shard_map/dot_general | solution.py:183
  164.2 12.8 %all-gather.14.cloned.1.call-done = bf16[1,1024,2048]{2,1,0:T(8,128)(2,1)} async-done(((bf16[1,256,2048]{2,1,0:T(8,128)(2,1)}), bf16[1,1024,2048]{2,1,0:T(8,128)(2,1)}) %all-gather.14.cloned.1.call-update) | async-done | bytes 4194320 | tf_op jit(solution)/shard_map/all_gather | solution.py:188
  177.0 8.6 %fusion.9 = bf16[384,2048]{1,0:T(8,128)(2,1)} fusion(bf16[1,1024,2048]{2,1,0:T(8,128)(2,1)} %all-gather.14.cloned.1.call-done, f32[384,1024]{1,0:T(8,128)} %fusion.7, bf16[384,2048]{1,0:T(8,128)(2,1)S(1)} %copy-done.3, bf16[1,2048,1024]{2,1,0:T(8,128)(2,1)} %all-gather.12.cloned.1.call-done), kind=kOutput, calls=%fused_computation.15 | convolution fusion | flops 3224371200 | bytes 13107200 | tf_op jit(solution)/shard_map/dot_general | solution.py:186
  185.6 3.7 %reshape.380 = bf16[64,6,2048]{2,1,0:T(8,128)(2,1)} reshape(bf16[384,2048]{1,0:T(8,128)(2,1)} %fusion.9) | data formatting | bytes 3145728 | tf_op jit(solution)/shard_map/reshape | solution.py:191
  189.3 10.9 %all-to-all-start.1 = ((bf16[64,6,2048]{2,1,0:T(8,128)(2,1)}), bf16[64,6,2048]{2,1,0:T(8,128)(2,1)}, u32[]{:S(2)}, u32[]{:S(2)}) async-start(bf16[64,6,2048]{2,1,0:T(8,128)(2,1)} %reshape.380), calls=%async_computation.2 | async-start | bytes 4194304 | tf_op jit(solution)/shard_map/all_to_all | solution.py:192
  200.7 50.6 %all-to-all-done.1 = bf16[64,6,2048]{2,1,0:T(8,128)(2,1)} async-done(((bf16[64,6,2048]{2,1,0:T(8,128)(2,1)}), bf16[64,6,2048]{2,1,0:T(8,128)(2,1)}, u32[]{:S(2)}, u32[]{:S(2)}) %all-to-all-start.1) | async-done | bytes 1572896 | tf_op jit(solution)/shard_map/all_to_all | solution.py:192
  251.3 2.6 reshape.381
  253.9 2.3 gather_fusion.1
  256.2 1.7 gather.15
  258.0 4.9 %multiply_reduce_fusion = bf16[128,2048]{1,0:T(8,128)(2,1)} fusion(bf16[128,2,2048]{2,1,0:T(2,128)(2,1)S(1)} %gather.15, pred[128,2]{1,0:T(8,128)(4,1)S(1)} %copy.76, f32[128,2]{1,0:T(8,128)S(1)} %copy.78), kind=kLoop, calls=%fused_computation.16 | loop fusion | flops 1835008 | bytes 1574144 | tf_op jit(solution)/shard_map/reduce_sum | solution.py:196
  (144 shorter events, 33.3 us)
Async XLA Ops:
  7.2 143.8 %copy-start = (bf16[256,2048]{1,0:T(8,128)(2,1)S(1)}, bf16[256,2048]{1,0:T(8,128)(2,1)}, u32[]{:S(2)}) copy-start(bf16[256,2048]{1,0:T(8,128)(2,1)} %param.23) | copy-start | bytes 3145732
  7.2 1.5 copy-start.8
  7.2 2.3 copy-start.2
  7.2 2.5 copy-start.10
  7.2 151.2 %all-gather.10.cloned.1.call-start = ((), (), s32[]{:S(2)}) async-start(), calls=%async_computation.4 | async-start | bytes 5242880 | tf_op jit(solution)/shard_map/all_gather | solution.py:182
  7.9 156.3 %all-gather.12.cloned.1.call-start = ((), (), s32[]{:S(2)}) async-start(), calls=%async_computation.5 | async-start | bytes 5242880 | tf_op jit(solution)/shard_map/all_gather | solution.py:182
  9.2 2.2 copy-start.6
  9.9 1.4 copy-start.15
  18.8 138.2 %all-to-all-start = ((bf16[64,6,2048]{2,1,0:T(8,128)(2,1)}), bf16[64,6,2048]{2,1,0:T(8,128)(2,1)S(1)}, u32[]{:S(2)}, u32[]{:S(2)}) async-start(bf16[64,6,2048]{2,1,0:T(8,128)(2,1)} %broadcast_select_fusion), calls=%async_computation.1 | async-start | bytes 4194304 | tf_op jit(solution)/shard_map/all_to_all | solution.py:179
  30.8 2.9 %copy-start.17 = (f32[512,2]{0,1:T(2,128)S(1)}, f32[512,2]{0,1:T(2,128)}, u32[]{:S(2)}) copy-start(f32[512,2]{0,1:T(2,128)} %param.24) | copy-start | bytes 12292
  30.9 3.3 %copy-start.28 = (u32[256]{0:T(256)S(1)}, u32[256]{0:T(256)}, u32[]{:S(2)}) copy-start(u32[256]{0:T(256)} %constant.123) | copy-start | bytes 3076
  30.9 4.5 %copy-start.25 = (f32[2048]{0:T(1024)S(1)}, f32[2048]{0:T(1024)}, u32[]{:S(2)}) copy-start(f32[2048]{0:T(1024)} %param.17) | copy-start | bytes 24580
  30.9 146.1 %all-gather.14.cloned.1.call-start = ((), (), s32[]{:S(2)}) async-start(), calls=%async_computation.6 | async-start | bytes 5242880 | tf_op jit(solution)/shard_map/all_gather | solution.py:188
  31.6 231.3 %reduce-scatter.2.cloned.1.call-start = ((), (), s32[]{:S(2)}) async-start(), calls=%async_computation.3 | async-start | bytes 2621440 | tf_op jit(solution)/shard_map/reduce_scatter | solution.py:145
  33.8 28.6 %copy-start.22 = (f32[512]{0:T(512)}, f32[512]{0:T(512)S(1)}, u32[]{:S(2)}) copy-start(f32[512]{0:T(512)S(1)} %add_rsqrt_fusion) | copy-start | bytes 6148
  66.0 2.9 %copy-start.11 = (f32[2]{0:T(128)}, f32[2]{0:T(128)S(1)}, u32[]{:S(2)}) copy-start(f32[2]{0:T(128)S(1)} %get-tuple-element.6) | copy-start | bytes 28
  66.0 2.9 %copy-start.13 = (f32[2]{0:T(128)}, f32[2]{0:T(128)S(1)}, u32[]{:S(2)}) copy-start(f32[2]{0:T(128)S(1)} %get-tuple-element.7) | copy-start | bytes 28
  66.1 2.9 %copy-start.21 = (f32[2]{0:T(128)}, f32[2]{0:T(128)S(1)}, u32[]{:S(2)}) copy-start(f32[2]{0:T(128)S(1)} %get-tuple-element.5) | copy-start | bytes 28
  72.4 2.7 %copy-start.20 = (f32[2]{0:T(128)}, f32[2]{0:T(128)S(1)}, u32[]{:S(2)}) copy-start(f32[2]{0:T(128)S(1)} %slice_convert_fusion.5) | copy-start | bytes 28
  91.9 45.3 %copy-start.12 = (f32[2]{0:T(128)S(1)}, f32[2]{0:T(128)}, u32[]{:S(2)}) copy-start(f32[2]{0:T(128)} %copy-done.11) | copy-start | bytes 28
  98.6 40.2 %copy-start.4 = (bf16[4,128,2,64]{3,1,2,0:T(8,128)(2,1)S(1)}, bf16[4,128,2,64]{3,1,2,0:T(8,128)(2,1)}, u32[]{:S(2)}) copy-start(bf16[4,128,2,64]{3,1,2,0:T(8,128)(2,1)} %copy.59) | copy-start | bytes 393220
  98.6 40.2 %copy-start.5 = (bf16[4,128,2,64]{3,1,2,0:T(8,128)(2,1)S(1)}, bf16[4,128,2,64]{3,1,2,0:T(8,128)(2,1)}, u32[]{:S(2)}) copy-start(bf16[4,128,2,64]{3,1,2,0:T(8,128)(2,1)} %copy.60) | copy-start | bytes 393220
  110.7 29.4 %copy-start.18 = (f32[4,2,128]{2,1,0:T(2,128)S(1)}, f32[4,2,128]{2,1,0:T(2,128)}, u32[]{:S(2)}) copy-start(f32[4,2,128]{2,1,0:T(2,128)} %copy.63) | copy-start | bytes 12292
  142.9 8.0 %copy-start.23 = (f32[512]{0:T(512)S(1)}, f32[512]{0:T(512)}, u32[]{:S(2)}) copy-start(f32[512]{0:T(512)} %copy-done.22) | copy-start | bytes 6148
  142.9 8.0 %copy-start.26 = (f32[2048]{0:T(1024)S(1)}, f32[2048]{0:T(1024)}, u32[]{:S(2)}) copy-start(f32[2048]{0:T(1024)} %param.17) | copy-start | bytes 24580
  142.9 8.0 %copy-start.27 = (f32[256]{0:T(256)S(1)}, f32[256]{0:T(256)}, u32[]{:S(2)}) copy-start(f32[256]{0:T(256)} %param.22) | copy-start | bytes 3076
  158.4 18.6 %copy-start.3 = (bf16[384,2048]{1,0:T(8,128)(2,1)S(1)}, bf16[384,2048]{1,0:T(8,128)(2,1)}, u32[]{:S(2)}) copy-start(bf16[384,2048]{1,0:T(8,128)(2,1)} %reshape.379) | copy-start | bytes 4718596
  189.3 10.9 %copy-start.7 = (s32[256]{0:T(256)S(1)}, s32[256]{0:T(256)}, u32[]{:S(2)}) copy-start(s32[256]{0:T(256)} %copy-done.6) | copy-start | bytes 3076
  189.3 11.1 %copy-start.9 = (s32[128,2]{0,1:T(2,128)S(1)}, s32[128,2]{0,1:T(2,128)}, u32[]{:S(2)}) copy-start(s32[128,2]{0,1:T(2,128)} %param.27) | copy-start | bytes 3076
  189.3 11.3 %copy-start.19 = (f32[128,2]{0,1:T(2,128)S(1)}, f32[128,2]{0,1:T(2,128)}, u32[]{:S(2)}) copy-start(f32[128,2]{0,1:T(2,128)} %param.28) | copy-start | bytes 3076
  189.3 11.4 %copy-start.16 = (s32[256,1]{0,1:T(1,128)S(1)}, s32[256,1]{0,1:T(1,128)}, u32[]{:S(2)}) copy-start(s32[256,1]{0,1:T(1,128)} %copy-done.15) | copy-start | bytes 3076
  189.3 62.0 %all-to-all-start.1 = ((bf16[64,6,2048]{2,1,0:T(8,128)(2,1)}), bf16[64,6,2048]{2,1,0:T(8,128)(2,1)}, u32[]{:S(2)}, u32[]{:S(2)}) async-start(bf16[64,6,2048]{2,1,0:T(8,128)(2,1)} %reshape.380), calls=%async_computation.2 | async-start | bytes 4194304 | tf_op jit(solution)/shard_map/all_to_all | solution.py:192
  (3 other events, 2.0 us)
Sparse Core Ops, SparseCore 0:
  9.8 56.8 all-gather.9
  68.5 54.8 all-gather.11
  125.2 51.7 all-gather.13
  180.0 32.6 reduce-scatter.1
where the time goes:
time: 270 us; the launch traced here: 269 us
  blocking collectives  66.2 us (25%)
  waiting for transfers between devices  65.4 us (24%)
  local copies, waits for them, and re-layouts  41.3 us (15%)
  matrix products  35.1 us (13%)
  other arithmetic  23.3 us (9%)
  starting transfers between devices  23.1 us (9%)
  between operations  15 us (6%)
    all_gather x5, blocking collectives, carried_in(): lax.all_gather(part.astype(kind), axis)  63.8 us
    all_to_all x1, waiting for transfers between devices, expert_half(): lax.all_to_all(results, EP, split_axis=0, concat_axis=0, tiled=True)  50.6 us
    all_gather x1, waiting for transfers between devices, expert_half(): lax.all_gather(expert_down[0], 'tp', axis=0, tiled=True)  12.8 us
    all_to_all x1, starting transfers between devices, expert_half(): lax.all_to_all(outgoing, EP, split_axis=0, concat_axis=0, tiled=True)  12 us
    all_to_all x1, starting transfers between devices, expert_half(): lax.all_to_all(results, EP, split_axis=0, concat_axis=0, tiled=True)  10.9 us
    concatenate x8, local copies, waits for them, and re-layouts, rotate(): jnp.concatenate([first_half * cosine - second * sine_part, first_half * s...  10.8 us
    dot_general x3, matrix products, project(): jnp.dot(normed, weight, preferred_element_type=jnp.float32)  8.88 us
    dot_general x1, matrix products, expert_half(): jnp.dot(hidden, lax.all_gather(expert_down[0], 'tp', axis=0, tiled=True),...  8.59 us
  transfers between devices with their start and end apart: 6, of which 2 were waited for; matrix products, arithmetic and copies ran while one was open for 37% of the time, Pallas kernels for 0%

commit v1 on v0

--- a/solution.py
+++ b/solution.py
@@ -1,6 +1,10 @@
+import functools
+
 import jax
 import jax.numpy as jnp
 from jax import lax
+from jax.experimental import pallas as pl
+from jax.experimental.pallas import tpu as pltpu
 from jax.sharding import Mesh
 from jax.sharding import PartitionSpec as P
 
@@ -152,48 +156,382 @@
     )
 
 
+CAP = 6
+MESH_ID = pl.DeviceIdType.MESH
+VMEM_LIMIT = 64 * 1024 * 1024 - 1024 * 1024
+
+
+def z_order(count):
+    steps = []
+    for k in range(1, count // 2 + 1):
+        steps.append(k)
+        if count - k != k:
+            steps.append(count - k)
+    return steps + [0]
+
+
+def place():
+    sizes = tuple(lax.axis_size(name) for name in EP)
+    spots = tuple(lax.axis_index(name) for name in EP)
+    return sizes, spots
+
+
+def for_each_peer(body):
+    (nz, nx, nc), (z, x, c) = place()
+
+    def step(i, carry):
+        tx = lax.rem(x + i // nc, nx)
+        tc = lax.rem(c + i % nc, nc)
+        for offset in z_order(nz):
+            tz = lax.rem(z + offset, nz)
+            call = functools.partial(
+                body, {"ep_0": tz, "ep_1": tx, "ep_2": tc}, (tz * nx + tx) * nc + tc
+            )
+            if offset == 0:
+                pl.when(i > 0)(call)
+            else:
+                call()
+        return carry
+
+    lax.fori_loop(0, nx * nc, step, 0)
+
+
+def remote(src, dst, send_sem, recv_sem, device):
+    return pltpu.make_async_remote_copy(
+        src_ref=src,
+        dst_ref=dst,
+        send_sem=send_sem,
+        recv_sem=recv_sem,
+        device_id=device,
+        device_id_type=MESH_ID,
+    )
+
+
+def wait_bytes(ref, sem):
+    pltpu.make_async_copy(ref, ref, sem).wait()
+
+
+def packed_ids(shape, dim, piece):
+    row = lax.broadcasted_iota(jnp.int32, shape, dim)
+    owner = (row // 8) * CAP
+    lane = row % 8
+    if piece is None:
+        return jnp.where(lane < CAP, owner + lane, -1)
+    return jnp.where(lane == 6, owner + piece, jnp.where(lane == 7, owner + 3 + piece, -1))
+
+
+def dot(a, b):
+    return jnp.dot(a, b, preferred_element_type=jnp.float32)
+
+
+def expert_kernel(
+    x_ref,
+    gain_ref,
+    routes_ref,
+    score_ref,
+    gate_hbm,
+    up_hbm,
+    down_hbm,
+    out_ref,
+    send_buf,
+    arrived,
+    rows,
+    gate_buf,
+    up_buf,
+    down_buf,
+    hidden,
+    part_send,
+    part_recv,
+    back_send,
+    back,
+    weigh,
+    dispatch_send,
+    dispatch_recv,
+    forward_send,
+    forward_recv,
+    weight_send,
+    weight_recv,
+    weight_local,
+    part_send_sem,
+    part_recv_sem,
+    back_send_sem,
+    back_recv_sem,
+    own_sem,
+):
+    (nz, nx, nc), (z, x, c) = place()
+    me = (z * nx + x) * nc + c
+    y = lax.axis_index("tp")
+    flip, mirror = y + 1 - 2 * (y % 2), 3 - y
+    weight_peer = {"tp": (1 - c) * flip + c * mirror}
+    token_peer = {"tp": (1 - c) * mirror + c * flip}
+    experts = nz * nx * nc
+    tokens, width = x_ref.shape
+    piece = width // 4
+    row_count = experts * CAP
+    group = min(32, experts)
+    group_count = experts // group
+
+    barrier = pltpu.get_barrier_semaphore()
+    for_each_peer(
+        lambda device, index: pl.semaphore_signal(
+            barrier, inc=1, device_id=device, device_id_type=MESH_ID
+        )
+    )
+    for peer in (weight_peer, token_peer):
+        pl.semaphore_signal(barrier, inc=1, device_id=peer, device_id_type=MESH_ID)
+    locals_ = []
+    for k, (source, target) in enumerate(
+        ((gate_hbm, gate_buf), (up_hbm, up_buf), (down_hbm, down_buf))
+    ):
+        locals_.append(pltpu.make_async_copy(source, target.at[0], weight_local.at[k]))
+        locals_[-1].start()
+    pl.semaphore_wait(barrier, experts + 1)
+
+    weights_out = [
+        remote(gate_hbm, gate_buf.at[1], weight_send.at[0], weight_recv.at[0], weight_peer),
+        remote(up_hbm, up_buf.at[1], weight_send.at[1], weight_recv.at[1], weight_peer),
+        remote(down_hbm, down_buf.at[1], weight_send.at[2], weight_recv.at[2], weight_peer),
+    ]
+    for copy in weights_out:
+        copy.start()
+
+    floats = x_ref[...].astype(jnp.float32)
+    scale = lax.rsqrt(jnp.mean(floats * floats, axis=-1, keepdims=True) + EPS)
+    normed = (floats * scale * gain_ref[...]).astype(jnp.bfloat16)
+
+    entries = 2 * tokens
+    routes = routes_ref[...]
+    named = lax.broadcasted_iota(jnp.int32, (experts, entries), 0) == routes
+    named_bf = jnp.where(named, 1.0, 0.0).astype(jnp.bfloat16)
+    earlier = lax.broadcasted_iota(jnp.int32, (entries, entries), 0) < lax.broadcasted_iota(
+        jnp.int32, (entries, entries), 1
+    )
+    prior = dot(named_bf, jnp.where(earlier, 1.0, 0.0).astype(jnp.bfloat16))
+    slot = jnp.sum(jnp.where(named, prior, 0.0), axis=0, keepdims=True).astype(jnp.int32)
+    target = routes * CAP + slot
+    first, second = target[:, :tokens], target[:, tokens:]
+    scores = score_ref[...]
+    shares = scores / jnp.sum(scores, axis=0, keepdims=True)
+
+    packed = (8 * experts, tokens)
+    ids = [packed_ids(packed, 0, j) for j in (None, 0, 1, 2)]
+    picks = [
+        jnp.where((i == first) | (i == second), 1.0, 0.0).astype(jnp.bfloat16) for i in ids
+    ]
+    last = normed[:, 3 * piece :]
+    for j in range(3):
+        chosen = jnp.concatenate([picks[0], picks[1 + j]], axis=1)
+        source = jnp.concatenate([normed[:, j * piece : (j + 1) * piece], last], axis=0)
+        send_buf[j] = dot(chosen, source).astype(jnp.bfloat16).reshape(experts, 8, piece)
+        for_each_peer(
+            lambda device, index, j=j: remote(
+                send_buf.at[j, index],
+                arrived.at[0, j, me],
+                dispatch_send.at[j],
+                dispatch_recv.at[j],
+                device,
+            ).start()
+        )
+        pltpu.make_async_copy(send_buf.at[j, me], arrived.at[0, j, me], own_sem.at[j]).start()
+
+    for n, i in enumerate(ids):
+        shared = jnp.where(i == first, shares[0:1], 0.0) + jnp.where(
+            i == second, shares[1:2], 0.0
+        )
+        turned = shared.T
+        high = turned.astype(jnp.bfloat16)
+        weigh[n, 0] = high
+        weigh[n, 1] = (turned - high.astype(jnp.float32)).astype(jnp.bfloat16)
+
+    shape = (group * CAP, group * 8)
+    spread = [
+        jnp.where(
+            packed_ids(shape, 1, j) == lax.broadcasted_iota(jnp.int32, shape, 0), 1.0, 0.0
+        ).astype(jnp.bfloat16)
+        for j in (None, 0, 1, 2)
+    ]
+    spread_last = jnp.concatenate(spread[1:], axis=1)
+
+    def unpack(side, j):
+        block = arrived[side, j].reshape(8 * experts, piece)
+        for g in range(group_count):
+            rows[side, g * group * CAP : (g + 1) * group * CAP, j * piece : (j + 1) * piece] = dot(
+                spread[0], block[g * group * 8 : (g + 1) * group * 8]
+            ).astype(jnp.bfloat16)
+
+    def unpack_last(side):
+        blocks = [arrived[side, j].reshape(8 * experts, piece) for j in range(3)]
+        for g in range(group_count):
+            stacked = jnp.concatenate(
+                [block[g * group * 8 : (g + 1) * group * 8] for block in blocks], axis=0
+            )
+            rows[side, g * group * CAP : (g + 1) * group * CAP, 3 * piece :] = dot(
+                spread_last, stacked
+            ).astype(jnp.bfloat16)
+
+    forwards = []
+    for j in range(3):
+        wait_bytes(send_buf.at[j, pl.ds(0, experts - 1)], dispatch_recv.at[j])
+        pltpu.make_async_copy(send_buf.at[j, me], arrived.at[0, j, me], own_sem.at[j]).wait()
+        forwards.append(
+            remote(
+                arrived.at[0, j],
+                arrived.at[1, j],
+                forward_send.at[j],
+                forward_recv.at[j],
+                token_peer,
+            )
+        )
+        forwards[-1].start()
+        unpack(0, j)
+    unpack_last(0)
+
+    def expand(side, half):
+        source = rows[side]
+        gate_part = dot(source, gate_buf[half])
+        up_part = dot(source, up_buf[half])
+        hidden[side, half] = (gate_part / (1.0 + jnp.exp(-gate_part)) * up_part).astype(
+            jnp.bfloat16
+        )
+
+    locals_[0].wait()
+    locals_[1].wait()
+    expand(0, 0)
+    for j in range(3):
+        forwards[j].wait_recv()
+        unpack(1, j)
+    unpack_last(1)
+    expand(1, 0)
+    weights_out[0].wait_recv()
+    weights_out[1].wait_recv()
+    expand(1, 1)
+
+    def contract(side, k):
+        columns = slice(k * piece, (k + 1) * piece)
+        return dot(hidden[side, 0], down_buf[0, :, columns]) + dot(
+            hidden[side, 1], down_buf[1, :, columns]
+        )
+
+    locals_[2].wait()
+    weights_out[2].wait_recv()
+    parts = {}
+    for k in (3, 0, 1, 2):
+        part_send[k] = contract(1, k).astype(jnp.bfloat16)
+        parts[k] = remote(
+            part_send.at[k], part_recv.at[k], part_send_sem.at[k], part_recv_sem.at[k], token_peer
+        )
+        parts[k].start()
+    expand(0, 1)
+
+    def total(k):
+        own = contract(0, k)
+        parts[k].wait_recv()
+        return (own + part_recv[k].astype(jnp.float32)).astype(jnp.bfloat16)
+
+    gather = [
+        jnp.where(
+            packed_ids((group * 8, group * CAP), 0, j)
+            == lax.broadcasted_iota(jnp.int32, (group * 8, group * CAP), 1),
+            1.0,
+            0.0,
+        ).astype(jnp.bfloat16)
+        for j in (None, 0, 1, 2)
+    ]
+    tail = total(3)
+    for j in range(3):
+        body = total(j)
+        for g in range(group_count):
+            span = slice(g * group * CAP, (g + 1) * group * CAP)
+            back_send[j, g * group : (g + 1) * group] = (
+                (dot(gather[0], body[span]) + dot(gather[1 + j], tail[span]))
+                .astype(jnp.bfloat16)
+                .reshape(group, 8, piece)
+            )
+        for_each_peer(
+            lambda device, index, j=j: remote(
+                back_send.at[j, index],
+                back.at[j, me],
+                back_send_sem.at[j],
+                back_recv_sem.at[j],
+                device,
+            ).start()
+        )
+        pltpu.make_async_copy(back_send.at[j, me], back.at[j, me], own_sem.at[j]).start()
+
+    rest = jnp.zeros((tokens, piece), jnp.float32)
+    for j in range(3):
+        wait_bytes(back_send.at[j, pl.ds(0, experts - 1)], back_recv_sem.at[j])
+        pltpu.make_async_copy(back_send.at[j, me], back.at[j, me], own_sem.at[j]).wait()
+        block = back[j].reshape(8 * experts, piece)
+        out_ref[:, j * piece : (j + 1) * piece] = (
+            dot(weigh[0, 0], block) + dot(weigh[0, 1], block)
+        ).astype(jnp.bfloat16)
+        rest = rest + dot(weigh[1 + j, 0], block) + dot(weigh[1 + j, 1], block)
+    out_ref[:, 3 * piece :] = rest.astype(jnp.bfloat16)
+
+    for copy in weights_out + forwards + list(parts.values()):
+        copy.wait_send()
+    for j in range(3):
+        wait_bytes(send_buf.at[j, pl.ds(0, experts - 1)], dispatch_send.at[j])
+        wait_bytes(back_send.at[j, pl.ds(0, experts - 1)], back_send_sem.at[j])
+
+
 def expert_half(
     expert_input, expert_gain, routes, route_weight, expert_gate, expert_up, expert_down
 ):
-    tok_count, top_count = routes.shape
+    tokens, width = expert_input.shape
     experts = lax.axis_size(EP)
-    capacity = max(2, 3 * tok_count * top_count // (2 * experts))
-    width = expert_input.shape[1]
-    normed = norm_rows(expert_input, expert_gain)
-    flat_routes = routes.reshape(-1)
-    entries = flat_routes.shape[0]
-    onehot = (flat_routes[:, None] == jnp.arange(experts, dtype=jnp.int32)[None, :]).astype(
-        jnp.bfloat16
-    )
-    before = (
-        lax.broadcasted_iota(jnp.int32, (entries, entries), 1)
-        < lax.broadcasted_iota(jnp.int32, (entries, entries), 0)
-    ).astype(jnp.bfloat16)
-    prior_count = jnp.dot(before, onehot, preferred_element_type=jnp.float32)
-    slot_index = jnp.sum(prior_count * onehot.astype(jnp.float32), axis=1).astype(jnp.int32)
-    target = flat_routes * capacity + slot_index
-    token_ids = jnp.arange(entries, dtype=jnp.int32) // top_count
-    slot_table = jnp.full((experts * capacity,), tok_count, jnp.int32).at[target].set(token_ids)
-    padded = jnp.concatenate([normed, jnp.zeros((1, width), jnp.bfloat16)], axis=0)
-    outgoing = jnp.take(padded, slot_table, axis=0).reshape(experts, capacity, width)
-    arrived = lax.all_to_all(outgoing, EP, split_axis=0, concat_axis=0, tiled=True)
-    sources = arrived.shape[0]
-    flat_rows = arrived.reshape(sources * capacity, width)
-    shard_piece = lax.all_gather((expert_gate[0], expert_up[0]), "tp", axis=1, tiled=True)
-    gate_part = jnp.dot(flat_rows, shard_piece[0], preferred_element_type=jnp.float32)
-    up_part = jnp.dot(flat_rows, shard_piece[1], preferred_element_type=jnp.float32)
-    hidden = (jax.nn.silu(gate_part) * up_part).astype(jnp.bfloat16)
-    reduced = jnp.dot(
-        hidden,
-        lax.all_gather(expert_down[0], "tp", axis=0, tiled=True),
-        preferred_element_type=jnp.float32,
-    )
-    results = reduced.astype(jnp.bfloat16).reshape(sources, capacity, width)
-    returned = lax.all_to_all(results, EP, split_axis=0, concat_axis=0, tiled=True)
-    picked = jnp.take(returned.reshape(experts * capacity, width), target, axis=0)
-    picked = picked.astype(jnp.float32).reshape(tok_count, top_count, width)
-    norm_weight = route_weight / jnp.sum(route_weight, axis=1, keepdims=True)
-    return jnp.sum(picked * norm_weight[:, :, None], axis=1).astype(jnp.bfloat16)
+    shard = expert_gate.shape[2]
+    piece = width // 4
+    row_count = experts * CAP
+    bf16 = jnp.bfloat16
+    vmem = pl.BlockSpec(memory_space=pltpu.VMEM)
+    anywhere = pl.BlockSpec(memory_space=pl.ANY)
+    dma = pltpu.SemaphoreType.DMA
+    return pl.pallas_call(
+        expert_kernel,
+        out_shape=jax.ShapeDtypeStruct((tokens, width), bf16),
+        in_specs=[vmem] * 4 + [anywhere] * 3,
+        out_specs=vmem,
+        scratch_shapes=[
+            pltpu.VMEM((3, experts, 8, piece), bf16),
+            pltpu.VMEM((2, 3, experts, 8, piece), bf16),
+            pltpu.VMEM((2, row_count, width), bf16),
+            pltpu.VMEM((2, width, shard), bf16),
+            pltpu.VMEM((2, width, shard), bf16),
+            pltpu.VMEM((2, shard, width), bf16),
+            pltpu.VMEM((2, 2, row_count, shard), bf16),
+            pltpu.VMEM((4, row_count, piece), bf16),
+            pltpu.VMEM((4, row_count, piece), bf16),
+            pltpu.VMEM((3, experts, 8, piece), bf16),
+            pltpu.VMEM((3, experts, 8, piece), bf16),
+            pltpu.VMEM((4, 2, tokens, 8 * experts), bf16),
+            dma((3,)),
+            dma((3,)),
+            dma((3,)),
+            dma((3,)),
+            dma((3,)),
+            dma((3,)),
+            dma((3,)),
+            dma((4,)),
+            dma((4,)),
+            dma((3,)),
+            dma((3,)),
+            dma((3,)),
+        ],
+        compiler_params=pltpu.CompilerParams(
+            collective_id=0, has_side_effects=True, vmem_limit_bytes=VMEM_LIMIT
+        ),
+        name="experts",
+    )(
+        expert_input,
+        expert_gain.reshape(1, width),
+        routes.T.reshape(1, -1),
+        route_weight.T,
+        expert_gate[0],
+        expert_up[0],
+        expert_down[0],
+    )
 
 
 def on_device(

time: 270 us -> 245 us (0.907)
  Pallas kernels: 0 us -> 129 us
  waiting for transfers between devices: 65.4 us -> 0.04 us
  local copies, waits for them, and re-layouts: 41.3 us -> 11 us
  starting transfers between devices: 23.1 us -> 0.04 us
  matrix products: 35.1 us -> 15.4 us
  other arithmetic: 23.3 us -> 4.48 us
    pallas_call x0 -> x1, Pallas kernels: none -> 129 us  [expert_half(): pl.pallas_call(expert_kernel, out_shape=jax.ShapeDtypeStruct((tokens, wid...]
    all_to_all x2 -> x0, waiting for transfers between devices: 50.6 us -> none  [the longest x1 50.6 us: expert_half(): lax.all_to_all(results, EP, split_axis=0, concat_axis=0, tiled=True)]
    all_to_all x2 -> x0, starting transfers between devices: 22.9 us -> none  [the longest x1 12 us: expert_half(): lax.all_to_all(outgoing, EP, split_axis=0, concat_axis=0, tiled=True)]
    dot_general x3 -> x0, matrix products: 14.6 us -> none  [the longest x1 8.59 us: expert_half(): jnp.dot(hidden, lax.all_gather(expert_down[0], 'tp', axis=0, tiled=True),...]
    all_gather x3 -> x0, waiting for transfers between devices: 12.8 us -> none  [the longest x1 12.8 us: expert_half(): lax.all_gather(expert_down[0], 'tp', axis=0, tiled=True)]
    gather x4 -> x0, local copies, waits for them, and re-layouts: 9.66 us -> none  [the longest x2 5.6 us: expert_half(): jnp.take(padded, slot_table, axis=0).reshape(experts, capacity, width)]
    concatenate x8, local copies, waits for them, and re-layouts: 10.8 us -> 2.4 us  [rotate(): jnp.concatenate([first_half * cosine - second * sine_part, first_half * s...]
    reshape x4 -> x0, local copies, waits for them, and re-layouts: 7.86 us -> none  [the longest x1 3.67 us: expert_half(): results = reduced.astype(jnp.bfloat16).reshape(sources, capacity, width)]
  transfers between devices with their start and end apart: 6 -> 1, of which waited for: 2 -> 0; matrix products, arithmetic and copies ran while one was open for 37% -> 0% of each run, Pallas kernels for 0% -> 53%
where the time goes in v1:
time: 245 us; the launch traced here: 243 us
  Pallas kernels  129 us (53%)
  blocking collectives  68.2 us (28%)
  matrix products  15.4 us (6%)
  between operations  15.1 us (6%)
  local copies, waits for them, and re-layouts  11 us (4%)
  other arithmetic  4.48 us (2%)
    pallas_call x1, Pallas kernels, expert_half(): pl.pallas_call(expert_kernel, out_shape=jax.ShapeDtypeStruct((tokens, wid...  129 us
    all_gather x5, blocking collectives, carried_in(): lax.all_gather(part.astype(kind), axis)  65.8 us
    dot_general x1, matrix products, mixer_half(): jnp.dot(mixer_hidden, output_weight, preferred_element_type=jnp.float32)  5.59 us
    dot_general x3, matrix products, project(): jnp.dot(normed, weight, preferred_element_type=jnp.float32)  5.15 us
  transfers between devices with their start and end apart: 1, of which 0 were waited for; matrix products, arithmetic and copies ran while one was open for 0% of the time, Pallas kernels for 53%

profile of v1, /device:TPU:2, one launch (start us, length us, event | category | flops | bytes accessed | tf_op | source)
XLA Modules:
  0.0 242.7 jit_solution(17814736514247672323)
XLA Ops:
  7.3 0.8 reshape.299
  8.3 0.2 slice_reduce_fusion
  8.5 1.3 dynamic-slice
  10.4 0.2 dynamic-update-slice
  10.6 2.4 %all-reduce = bf16[4]{0:T(256)(128)(2,1)S(1)} all-reduce(bf16[4]{0:T(256)(128)(2,1)S(1)} %dynamic-update-slice), channel_id=2, replica_groups=mesh['ep_0'=8,'ep_1'=4,'ep_2'=2,'tp'=4] {'ep_2'}, use_global_device_ids=true, to_apply=%add | all-reduce | flops 4 | bytes 16
  13.2 9.2 %all-gather.1 = bf16[4,1,2]{2,1,0:T(2,128)(2,1)S(1)} all-gather(bf16[1,1,2]{2,1,0:T(2,128)(2,1)S(1)} %convert_bitcast_fusion), channel_id=1, replica_groups=mesh['ep_0'=8,'ep_1'=4,'ep_2'=2,'tp'=4] {'ep_1'}, dimensions={0}, use_global_device_ids=true | all-gather | bytes 20 | tf_op jit(solution)/shard_map/all_gather | solution.py:31
  22.4 17.8 %all-gather.2 = bf16[8,1,2]{2,1,0:T(2,128)(2,1)S(1)} all-gather(bf16[1,1,2]{2,1,0:T(2,128)(2,1)S(1)} %fusion.51), channel_id=1, replica_groups=mesh['ep_0'=8,'ep_1'=4,'ep_2'=2,'tp'=4] {'ep_0'}, dimensions={0}, use_global_device_ids=true | all-gather | bytes 36 | tf_op jit(solution)/shard_map/all_gather | solution.py:31
  40.4 0.2 slice_reduce_fusion.5
  40.6 2.1 fusion
  42.8 2.2 convolution_convert_fusion.3
  45.1 0.9 convolution_convert_fusion.2
  46.1 0.5 multiply_cosine_fusion
  46.8 0.9 copy.36
  47.7 0.9 copy.37
  48.7 0.2 copy.39
  49.0 0.2 copy.38
  49.2 2.0 convolution_convert_fusion.4
  51.2 0.8 reshape.294
  52.0 0.2 fusion.9
  52.2 1.4 fusion.17
  53.7 2.0 all_gather.27
  55.9 11.4 %all_gather.28 = bf16[4,2,128,128]{3,2,1,0:T(8,128)(2,1)S(1)} all-gather(bf16[1,2,128,128]{3,2,1,0:T(8,128)(2,1)S(1)} %fusion.38), channel_id=1, replica_groups=mesh['ep_0'=8,'ep_1'=4,'ep_2'=2,'tp'=4] {'ep_1'}, dimensions={0}, use_global_device_ids=true | all-gather | bytes 327680 | tf_op jit(solution)/shard_map/all_gather | solution.py:31
  67.5 25.3 %all_gather.29 = bf16[8,2,128,128]{3,2,1,0:T(8,128)(2,1)S(1)} all-gather(bf16[1,2,128,128]{3,2,1,0:T(8,128)(2,1)S(1)} %fusion.37), channel_id=1, replica_groups=mesh['ep_0'=8,'ep_1'=4,'ep_2'=2,'tp'=4] {'ep_0'}, dimensions={0}, use_global_device_ids=true | all-gather | bytes 589824 | tf_op jit(solution)/shard_map/all_gather | solution.py:31
  92.8 0.4 multiply_add_fusion.1
  93.3 1.3 convolution_bitcast_fusion.1
  94.6 1.8 fusion.67
  96.4 1.0 copy.48
  97.8 0.6 sub.54
  98.4 1.4 mul.536
  99.8 5.6 %convolution_convert_fusion = bf16[512,2048]{1,0:T(8,128)(2,1)} fusion(bf16[256,2048]{1,0:T(8,128)(2,1)} %param.23, f32[64,8,2,128]{3,2,1,0:T(2,128)} %bitcast.144, f32[64,8,2,128]{3,2,1,0:T(2,128)S(1)} %bitcast.143, f32[64,8,2,128]{3,2,1,0:T(2,128)} %bitcast.145, bf16[2048,256]{1,0:T(8,128)(2,1)} %param.21, f32[256]{0:T(256)S(1)} %copy-done.6, ...), kind=kOutput, calls=%fused_computation.5 | convolution fusion | flops 1080426496 | bytes 7875584 | tf_op jit(solution)/shard_map/dot_general | solution.py:150
  105.4 128.5 %experts.1 = bf16[128,2048]{1,0:T(8,128)(2,1)} custom-call(bf16[128,2048]{1,0:T(8,128)(2,1)} %x_ref.1, f32[1,2048]{1,0:T(1,128)} %bitcast.148, s32[1,256]{1,0:T(1,128)} %bitcast.149, f32[2,128]{1,0:T(2,128)} %bitcast.150, bf16[2048,256]{1,0:T(8,128)(2,1)} %bitcast.140, bf16[2048,256]{1,0:T(8,128)(2,1)} %bitcast.141, bf16[256,2048]{1,0:T(8,128)(2,1)} %bitcast.142), custom_call_target="tpu_custom_call" | custom-call | tf_op jit(solution)/shard_map/experts/pallas_call | solution.py:491
  234.0 1.9 copy.73
  (52 shorter events, 1.9 us)
Async XLA Ops:
  7.2 35.6 %copy-start = (bf16[512,2048]{1,0:T(8,128)(2,1)S(1)}, bf16[512,2048]{1,0:T(8,128)(2,1)}, u32[]{:S(2)}) copy-start(bf16[512,2048]{1,0:T(8,128)(2,1)} %param.16) | copy-start | bytes 6291460
  7.2 35.6 %copy-start.5 = (f32[2048]{0:T(1024)S(1)}, f32[2048]{0:T(1024)}, u32[]{:S(2)}) copy-start(f32[2048]{0:T(1024)} %param.17) | copy-start | bytes 24580
  7.2 226.8 %reduce-scatter.2.cloned.1.call-start = ((), (), s32[]{:S(2)}) async-start(), calls=%async_computation.1 | async-start | bytes 2621440 | tf_op jit(solution)/shard_map/reduce_scatter | solution.py:149
  42.7 2.3 copy-start.4
  53.6 39.7 %copy-start.2 = (bf16[4,128,2,64]{3,1,2,0:T(8,128)(2,1)S(1)}, bf16[4,128,2,64]{3,1,2,0:T(8,128)(2,1)}, u32[]{:S(2)}) copy-start(bf16[4,128,2,64]{3,1,2,0:T(8,128)(2,1)} %copy.36) | copy-start | bytes 393220
  53.6 39.7 %copy-start.3 = (bf16[4,128,2,64]{3,1,2,0:T(8,128)(2,1)S(1)}, bf16[4,128,2,64]{3,1,2,0:T(8,128)(2,1)}, u32[]{:S(2)}) copy-start(bf16[4,128,2,64]{3,1,2,0:T(8,128)(2,1)} %copy.37) | copy-start | bytes 393220
  67.4 27.2 %copy-start.1 = (bf16[4,128,2,128]{3,2,1,0:T(2,128)(2,1)S(1)}, bf16[4,128,2,128]{3,2,1,0:T(2,128)(2,1)}, u32[]{:S(2)}) copy-start(bf16[4,128,2,128]{3,2,1,0:T(2,128)(2,1)} %reshape.294) | copy-start | bytes 786436
  96.4 3.4 %copy-start.6 = (f32[256]{0:T(256)S(1)}, f32[256]{0:T(256)}, u32[]{:S(2)}) copy-start(f32[256]{0:T(256)} %param.22) | copy-start | bytes 3076
Sparse Core Ops, SparseCore 0:
  105.6 44.0 reduce-scatter.1

commit v2 on v1

--- a/solution.py
+++ b/solution.py
@@ -11,152 +11,9 @@
 BLOCK = 128
 EP = ("ep_0", "ep_1", "ep_2")
 EP_TP = ("ep_0", "ep_1", "ep_2", "tp")
-
-
 EPS = 1e-06
-
-
-def filled_with(x, identity):
-    return jax.tree.map(
-        lambda part, zero: jnp.zeros_like(part) + jnp.asarray(zero, part.dtype), x, identity
-    )
-
-
-def carried_in(x, axes, combine, identity):
-    before = start = filled_with(x, identity)
-    running = x
-    for axis in reversed(axes):
-        peers, position = (lax.axis_size(axis), lax.axis_index(axis))
-        pieces = jax.tree.map(
-            lambda part, kind: lax.all_gather(part.astype(kind), axis),
-            running,
-            (jnp.bfloat16, jnp.bfloat16),
-        )
-        inside, running = (start, start)
-        for k in range(peers):
-            passed = k < position
-            running = combine(
-                running, jax.tree.map(lambda part, own: part[k].astype(own.dtype), pieces, x)
-            )
-            inside = jax.tree.map(lambda new, old: jnp.where(passed, new, old), running, inside)
-        before = combine(inside, before)
-    return before
-
-
-def norm_rows(values, gain):
-    floats = values.astype(jnp.float32)
-    scale = lax.rsqrt(jnp.mean(floats * floats, axis=-1, keepdims=True) + EPS)
-    return (floats * scale * gain).astype(jnp.bfloat16)
-
-
-def rotate(values, position):
-    half_dim = values.shape[-1] // 2
-    frequency = 10000.0 ** (-jnp.arange(half_dim, dtype=jnp.float32) / half_dim)
-    angles = position.astype(jnp.float32)[:, None] * frequency[None, :]
-    cosine = jnp.cos(angles)[:, None, :]
-    sine_part = jnp.sin(angles)[:, None, :]
-    first_half = values[..., :half_dim]
-    second = values[..., half_dim:]
-    return jnp.concatenate(
-        [first_half * cosine - second * sine_part, first_half * sine_part + second * cosine],
-        axis=-1,
-    )
-
-
-def chain_pair(earlier, following):
-    return (earlier[0] * following[0], following[0][:, None, None] * earlier[1] + following[1])
-
-
-def mixer_half(
-    mixer_input,
-    mixer_gain,
-    query_weight,
-    key_weight,
-    value_weight,
-    gate_weight,
-    head_gain,
-    output_weight,
-    log_decay,
-):
-    row_count = mixer_input.shape[0]
-    head_count = log_decay.shape[1]
-    mix_width = query_weight.shape[1]
-    head_dim = mix_width // head_count
-    normed = norm_rows(mixer_input, mixer_gain)
-
-    def project(weight):
-        return jnp.dot(normed, weight, preferred_element_type=jnp.float32).astype(jnp.bfloat16)
-
-    queries = project(query_weight)
-    keys_raw = project(key_weight)
-    values_new = project(value_weight)
-    gate_raw = project(gate_weight)
-    position = lax.axis_index(EP) * row_count + jnp.arange(row_count, dtype=jnp.int32)
-    q_rot = rotate(
-        queries.astype(jnp.float32).reshape(row_count, head_count, head_dim), position
-    ).astype(jnp.bfloat16)
-    k_rot = (
-        rotate(keys_raw.astype(jnp.float32).reshape(row_count, head_count, head_dim), position)
-        * head_dim ** (-0.5)
-    ).astype(jnp.bfloat16)
-    block_count = row_count // BLOCK
-    q_blocks = q_rot.reshape(block_count, BLOCK, head_count, head_dim)
-    k_blocks = k_rot.reshape(block_count, BLOCK, head_count, head_dim)
-    v_blocks = values_new.reshape(block_count, BLOCK, head_count, head_dim)
-    log_steps = log_decay.reshape(block_count, BLOCK, head_count)
-    row_ids = lax.broadcasted_iota(jnp.int32, (BLOCK, BLOCK), 0)
-    col_ids = lax.broadcasted_iota(jnp.int32, (BLOCK, BLOCK), 1)
-    lower_mask = col_ids <= row_ids
-    cumulative = jnp.einsum("ij,bjh->bhi", lower_mask.astype(jnp.float32), log_steps)
-    block_total = cumulative[:, :, -1]
-    differences = cumulative[:, :, :, None] - cumulative[:, :, None, :]
-    decays = jnp.where(lower_mask, jnp.exp(jnp.where(lower_mask, differences, 0.0)), 0.0)
-    scores = jnp.einsum("bihd,bjhd->bhij", q_blocks, k_blocks, preferred_element_type=jnp.float32)
-    weights = (scores * decays).astype(jnp.bfloat16)
-    inner_term = jnp.einsum(
-        "bhij,bjhe->bihe", weights, v_blocks, preferred_element_type=jnp.float32
-    )
-    key_scale = jnp.exp(block_total[:, :, None] - cumulative)
-    updates = jnp.einsum(
-        "bhj,bjhd,bjhe->bhde", key_scale, k_blocks.astype(jnp.float32), v_blocks.astype(jnp.float32)
-    )
-    factor = jnp.exp(block_total)
-    local_state = jnp.zeros((head_count, head_dim, head_dim), jnp.float32)
-    for block_index in range(block_count):
-        local_state = factor[block_index][:, None, None] * local_state + updates[block_index]
-    entering = carried_in(
-        (jnp.exp(jnp.sum(block_total, axis=0)), local_state),
-        EP,
-        chain_pair,
-        (jnp.ones((head_count,), jnp.float32), jnp.zeros_like(local_state)),
-    )
-    carry_state = entering[1]
-    starts = []
-    for block_index in range(block_count):
-        starts.append(carry_state)
-        carry_state = factor[block_index][:, None, None] * carry_state + updates[block_index]
-    carried = jnp.stack(starts)
-    cross_term = jnp.einsum(
-        "bhi,bihd,bhde->bihe", jnp.exp(cumulative), q_blocks.astype(jnp.float32), carried
-    )
-    retained = (inner_term + cross_term).reshape(row_count, head_count, head_dim)
-    centre = jnp.mean(retained, axis=-1, keepdims=True)
-    spread = jnp.mean(jnp.square(retained - centre), axis=-1, keepdims=True)
-    scaled = (retained - centre) * lax.rsqrt(spread + EPS) * head_gain.reshape(head_count, head_dim)
-    mixer_hidden = (
-        scaled.reshape(row_count, mix_width) * jax.nn.silu(gate_raw.astype(jnp.float32))
-    ).astype(jnp.bfloat16)
-    return lax.psum_scatter(
-        jnp.dot(mixer_hidden, output_weight, preferred_element_type=jnp.float32).astype(
-            jnp.bfloat16
-        ),
-        "tp",
-        scatter_dimension=0,
-        tiled=True,
-    )
-
-
 CAP = 6
+HEAD = 128
 MESH_ID = pl.DeviceIdType.MESH
 VMEM_LIMIT = 64 * 1024 * 1024 - 1024 * 1024
 
@@ -224,7 +81,99 @@
     return jnp.dot(a, b, preferred_element_type=jnp.float32)
 
 
-def expert_kernel(
+def dot_t(a, b, dims):
+    return lax.dot_general(a, b, (dims, ((), ())), preferred_element_type=jnp.float32)
+
+
+def project_rows(mx_buf, mx_gain, mixer_weights, cos_ref, sin_ref, q_buf, k_buf, v_buf, g_buf):
+    row_count, width = mx_buf.shape
+    step_rows = min(256, row_count)
+    heads = q_buf.shape[1] // HEAD
+
+    def step(i, carry):
+        span = pl.ds(pl.multiple_of(i * step_rows, step_rows), step_rows)
+        floats = mx_buf[span, :].astype(jnp.float32)
+        scale = lax.rsqrt(jnp.mean(floats * floats, axis=-1, keepdims=True) + EPS)
+        normed = (floats * scale * mx_gain[...]).astype(jnp.bfloat16)
+        cosine, sine = cos_ref[span, :], sin_ref[span, :]
+        for n, target in enumerate((q_buf, k_buf, v_buf, g_buf)):
+            raw = dot(normed, mixer_weights[n]).astype(jnp.bfloat16)
+            if n >= 2:
+                target[span, :] = raw
+                continue
+            for h in range(heads):
+                part = raw[:, h * HEAD : (h + 1) * HEAD].astype(jnp.float32)
+                swapped = jnp.concatenate([part[:, HEAD // 2 :], part[:, : HEAD // 2]], axis=1)
+                turned = part * cosine + swapped * sine
+                if n == 1:
+                    turned = turned * HEAD ** (-0.5)
+                target[span, h * HEAD : (h + 1) * HEAD] = turned.astype(jnp.bfloat16)
+        return carry
+
+    lax.fori_loop(0, row_count // step_rows, step, 0)
+
+
+def scan_blocks(logs_ref, log_rows_ref, q_buf, k_buf, v_buf, inner_buf, update_buf, decay_buf):
+    block_count = q_buf.shape[0] // BLOCK
+    heads = q_buf.shape[1] // HEAD
+    row_ids = lax.broadcasted_iota(jnp.int32, (BLOCK, BLOCK), 0)
+    col_ids = lax.broadcasted_iota(jnp.int32, (BLOCK, BLOCK), 1)
+    lower, upper = col_ids <= row_ids, row_ids <= col_ids
+
+    def step(b, carry):
+        span = pl.ds(pl.multiple_of(b * BLOCK, BLOCK), BLOCK)
+        tall, wide = logs_ref[span, :], log_rows_ref[b]
+        for h in range(heads):
+            lanes = slice(h * HEAD, (h + 1) * HEAD)
+            cum_col = jnp.sum(jnp.where(lower, wide[h : h + 1, :], 0.0), axis=1, keepdims=True)
+            cum_row = jnp.sum(jnp.where(upper, tall[:, h : h + 1], 0.0), axis=0, keepdims=True)
+            total = jnp.sum(wide[h : h + 1, :], axis=1, keepdims=True)
+            q, k, v = q_buf[span, lanes], k_buf[span, lanes], v_buf[span, lanes]
+            scaled = (k.astype(jnp.float32) * jnp.exp(total - cum_col)).astype(jnp.bfloat16)
+            update_buf[b, h] = dot_t(scaled, v, ((0,), (0,)))
+            decay_buf[b, h] = jnp.broadcast_to(total, (8, HEAD))
+            decays = jnp.where(lower, jnp.exp(jnp.where(lower, cum_col - cum_row, 0.0)), 0.0)
+            scores = dot_t(q, k, ((1,), (1,)))
+            inner_buf[span, lanes] = dot((scores * decays).astype(jnp.bfloat16), v)
+            q_buf[span, lanes] = (q.astype(jnp.float32) * jnp.exp(cum_col)).astype(jnp.bfloat16)
+        return carry
+
+    lax.fori_loop(0, block_count, step, 0)
+
+
+def finish_blocks(
+    entering, q_buf, g_buf, inner_buf, update_buf, decay_buf, head_gain, out_weight, out_buf
+):
+    block_count = q_buf.shape[0] // BLOCK
+    heads = q_buf.shape[1] // HEAD
+
+    def step(b, states):
+        span = pl.ds(pl.multiple_of(b * BLOCK, BLOCK), BLOCK)
+        following, hidden = [], []
+        for h in range(heads):
+            lanes = slice(h * HEAD, (h + 1) * HEAD)
+            state = states[h]
+            retained = inner_buf[span, lanes] + dot(q_buf[span, lanes], state.astype(jnp.bfloat16))
+            factor = jnp.exp(decay_buf[b, h][0:1])
+            following.append(factor * state + update_buf[b, h])
+            centred = retained - jnp.mean(retained, axis=-1, keepdims=True)
+            spread = jnp.mean(centred * centred, axis=-1, keepdims=True)
+            gate = g_buf[span, lanes].astype(jnp.float32)
+            hidden.append(
+                (
+                    centred
+                    * lax.rsqrt(spread + EPS)
+                    * head_gain[:, lanes]
+                    * (gate / (1.0 + jnp.exp(-gate)))
+                ).astype(jnp.bfloat16)
+            )
+        out_buf[span, :] = dot(jnp.concatenate(hidden, axis=1), out_weight[...]).astype(jnp.bfloat16)
+        return tuple(following)
+
+    lax.fori_loop(0, block_count, step, tuple(entering))
+
+
+def layer_kernel(
     x_ref,
     gain_ref,
     routes_ref,
@@ -232,6 +181,19 @@
     gate_hbm,
     up_hbm,
     down_hbm,
+    mx_hbm,
+    mx_gain,
+    q_hbm,
+    k_hbm,
+    v_hbm,
+    g_hbm,
+    head_gain,
+    o_hbm,
+    logs_ref,
+    log_rows_ref,
+    cos_ref,
+    sin_ref,
+    mixed_ref,
     out_ref,
     send_buf,
     arrived,
@@ -257,6 +219,33 @@
     back_send_sem,
     back_recv_sem,
     own_sem,
+    mx_buf,
+    mixer_weights,
+    o_buf,
+    q_buf,
+    k_buf,
+    v_buf,
+    g_buf,
+    inner_buf,
+    update_buf,
+    decay_buf,
+    mix_buf,
+    state_send,
+    state_got,
+    slab_send,
+    slab_got,
+    enter_send,
+    enter_got,
+    relay_got,
+    side_got,
+    load_sem,
+    state_sems,
+    relay_send,
+    relay_recv,
+    direct_send,
+    direct_recv,
+    summed_send,
+    summed_recv,
 ):
     (nz, nx, nc), (z, x, c) = place()
     me = (z * nx + x) * nc + c
@@ -271,6 +260,13 @@
     group = min(32, experts)
     group_count = experts // group
 
+    slab = nx * nc
+    spot = x * nc + c
+    loads = [pltpu.make_async_copy(mx_hbm, mx_buf, load_sem.at[0])]
+    for n, source in enumerate((q_hbm, k_hbm, v_hbm, g_hbm)):
+        loads.append(pltpu.make_async_copy(source, mixer_weights.at[n], load_sem.at[1 + n]))
+    loads.append(pltpu.make_async_copy(o_hbm, o_buf, load_sem.at[5]))
+
     barrier = pltpu.get_barrier_semaphore()
     for_each_peer(
         lambda device, index: pl.semaphore_signal(
@@ -285,6 +281,8 @@
     ):
         locals_.append(pltpu.make_async_copy(source, target.at[0], weight_local.at[k]))
         locals_[-1].start()
+    for load in loads:
+        load.start()
     pl.semaphore_wait(barrier, experts + 1)
 
     weights_out = [
@@ -334,6 +332,37 @@
         )
         pltpu.make_async_copy(send_buf.at[j, me], arrived.at[0, j, me], own_sem.at[j]).start()
 
+    for load in loads:
+        load.wait()
+    project_rows(mx_buf, mx_gain, mixer_weights, cos_ref, sin_ref, q_buf, k_buf, v_buf, g_buf)
+    scan_blocks(logs_ref, log_rows_ref, q_buf, k_buf, v_buf, inner_buf, update_buf, decay_buf)
+    block_count, heads = update_buf.shape[:2]
+    share = HEAD // slab
+    for h in range(heads):
+        state = update_buf[0, h]
+        decayed = decay_buf[0, h]
+        for b in range(1, block_count):
+            state = jnp.exp(decay_buf[b, h][0:1]) * state + update_buf[b, h]
+            decayed = decayed + decay_buf[b, h]
+        for n in range(slab):
+            state_send[n, h, :share] = state[n * share : (n + 1) * share]
+            state_send[n, h, share:] = decayed
+
+    def for_slab(body):
+        def step(i, carry):
+            n = lax.rem(spot + i, slab)
+            body(n, {"ep_1": n // nc, "ep_2": n % nc})
+            return carry
+
+        lax.fori_loop(1, slab, step, 0)
+
+    for_slab(
+        lambda n, device: remote(
+            state_send.at[n], state_got.at[spot], state_sems.at[0], state_sems.at[1], device
+        ).start()
+    )
+    state_got[spot] = state_send[spot]
+
     for n, i in enumerate(ids):
         shared = jnp.where(i == first, shares[0:1], 0.0) + jnp.where(
             i == second, shares[1:2], 0.0
@@ -369,8 +398,37 @@
                 spread_last, stacked
             ).astype(jnp.bfloat16)
 
+    wait_bytes(state_send.at[pl.ds(0, slab - 1)], state_sems.at[1])
+    running = [jnp.zeros((share, HEAD), jnp.float32)] * heads
+    decayed = [jnp.zeros((1, HEAD), jnp.float32)] * heads
+    prefixes, prefix_decays = [], []
+    for n in range(slab):
+        prefixes.append(list(running))
+        prefix_decays.append(list(decayed))
+        for h in range(heads):
+            log_total = state_got[n, h, share : share + 1]
+            running[h] = jnp.exp(log_total) * running[h] + state_got[n, h, :share]
+            decayed[h] = decayed[h] + log_total
+    for h in range(heads):
+        slab_send[h, :share] = running[h]
+        slab_send[h, share:] = jnp.broadcast_to(decayed[h], (8, HEAD))
+
+    def z_step(i, carry):
+        remote(
+            slab_send,
+            slab_got.at[z],
+            state_sems.at[2],
+            state_sems.at[3],
+            {"ep_0": lax.rem(z + i, nz)},
+        ).start()
+        return carry
+
+    lax.fori_loop(1, nz, z_step, 0)
+    slab_got[z] = slab_send[...]
+
     forwards = []
-    for j in range(3):
+
+    def forward(j):
         wait_bytes(send_buf.at[j, pl.ds(0, experts - 1)], dispatch_recv.at[j])
         pltpu.make_async_copy(send_buf.at[j, me], arrived.at[0, j, me], own_sem.at[j]).wait()
         forwards.append(
@@ -384,6 +442,34 @@
         )
         forwards[-1].start()
         unpack(0, j)
+
+    forward(0)
+    wait_bytes(slab_got.at[pl.ds(0, nz - 1)], state_sems.at[3])
+    for h in range(heads):
+        entry = jnp.zeros((share, HEAD), jnp.float32)
+        for n in range(nz):
+            entry = jnp.where(
+                n < z,
+                jnp.exp(slab_got[n, h, share : share + 1]) * entry + slab_got[n, h, :share],
+                entry,
+            )
+        for n in range(slab):
+            enter_send[n, h] = jnp.exp(prefix_decays[n][h]) * entry + prefixes[n][h]
+    for_slab(
+        lambda n, device: remote(
+            enter_send.at[n], enter_got.at[spot], state_sems.at[4], state_sems.at[5], device
+        ).start()
+    )
+    enter_got[spot] = enter_send[spot]
+    wait_bytes(enter_send.at[pl.ds(0, slab - 1)], state_sems.at[5])
+    entering = [
+        jnp.concatenate([enter_got[n, h] for n in range(slab)], axis=0) for h in range(heads)
+    ]
+    forward(1)
+    finish_blocks(
+        entering, q_buf, g_buf, inner_buf, update_buf, decay_buf, head_gain, o_buf, mix_buf
+    )
+    forward(2)
     unpack_last(0)
 
     def expand(side, half):
@@ -421,6 +507,38 @@
             part_send.at[k], part_recv.at[k], part_send_sem.at[k], part_recv_sem.at[k], token_peer
         )
         parts[k].start()
+
+    unit = mix_buf.shape[0] // 4
+    half = width // 2
+    right, left = lax.rem(y + 1, 4), lax.rem(y + 3, 4)
+
+    def slot_of(owner):
+        return pl.ds(pl.multiple_of(owner * unit, unit), unit)
+
+    opposite = slot_of(lax.rem(y + 2, 4))
+    sides = ((right, slice(0, half), slice(half, width)), (left, slice(half, width), slice(0, half)))
+    directs = []
+    for n, (peer, relayed, plain) in enumerate(sides):
+        directs.append(
+            remote(
+                mix_buf.at[opposite, relayed],
+                relay_got.at[n],
+                relay_send.at[n],
+                relay_recv.at[n],
+                {"tp": peer},
+            )
+        )
+        directs.append(
+            remote(
+                mix_buf.at[slot_of(peer), plain],
+                side_got.at[n, :, plain],
+                direct_send.at[n],
+                direct_recv.at[n],
+                {"tp": peer},
+            )
+        )
+    for copy in directs:
+        copy.start()
     expand(0, 1)
 
     def total(k):
@@ -458,6 +576,31 @@
         )
         pltpu.make_async_copy(back_send.at[j, me], back.at[j, me], own_sem.at[j]).start()
 
+    summed = []
+    for n, (peer, relayed, plain) in enumerate(sides):
+        directs[2 * n].wait_recv()
+        mix_buf[slot_of(peer), relayed] = (
+            mix_buf[slot_of(peer), relayed].astype(jnp.float32) + relay_got[n].astype(jnp.float32)
+        ).astype(jnp.bfloat16)
+        summed.append(
+            remote(
+                mix_buf.at[slot_of(peer), relayed],
+                side_got.at[n, :, relayed],
+                summed_send.at[n],
+                summed_recv.at[n],
+                {"tp": peer},
+            )
+        )
+        summed[-1].start()
+    for n in range(2):
+        directs[2 * n + 1].wait_recv()
+        summed[n].wait_recv()
+    mixed_ref[...] = (
+        mix_buf[slot_of(y), :].astype(jnp.float32)
+        + side_got[0].astype(jnp.float32)
+        + side_got[1].astype(jnp.float32)
+    ).astype(jnp.bfloat16)
+
     rest = jnp.zeros((tokens, piece), jnp.float32)
     for j in range(3):
         wait_bytes(back_send.at[j, pl.ds(0, experts - 1)], back_recv_sem.at[j])
@@ -469,69 +612,16 @@
         rest = rest + dot(weigh[1 + j, 0], block) + dot(weigh[1 + j, 1], block)
     out_ref[:, 3 * piece :] = rest.astype(jnp.bfloat16)
 
-    for copy in weights_out + forwards + list(parts.values()):
+    for copy in weights_out + forwards + list(parts.values()) + directs + summed:
         copy.wait_send()
     for j in range(3):
         wait_bytes(send_buf.at[j, pl.ds(0, experts - 1)], dispatch_send.at[j])
         wait_bytes(back_send.at[j, pl.ds(0, experts - 1)], back_send_sem.at[j])
 
 
-def expert_half(
-    expert_input, expert_gain, routes, route_weight, expert_gate, expert_up, expert_down
-):
-    tokens, width = expert_input.shape
-    experts = lax.axis_size(EP)
-    shard = expert_gate.shape[2]
-    piece = width // 4
-    row_count = experts * CAP
-    bf16 = jnp.bfloat16
-    vmem = pl.BlockSpec(memory_space=pltpu.VMEM)
-    anywhere = pl.BlockSpec(memory_space=pl.ANY)
-    dma = pltpu.SemaphoreType.DMA
-    return pl.pallas_call(
-        expert_kernel,
-        out_shape=jax.ShapeDtypeStruct((tokens, width), bf16),
-        in_specs=[vmem] * 4 + [anywhere] * 3,
-        out_specs=vmem,
-        scratch_shapes=[
-            pltpu.VMEM((3, experts, 8, piece), bf16),
-            pltpu.VMEM((2, 3, experts, 8, piece), bf16),
-            pltpu.VMEM((2, row_count, width), bf16),
-            pltpu.VMEM((2, width, shard), bf16),
-            pltpu.VMEM((2, width, shard), bf16),
-            pltpu.VMEM((2, shard, width), bf16),
-            pltpu.VMEM((2, 2, row_count, shard), bf16),
-            pltpu.VMEM((4, row_count, piece), bf16),
-            pltpu.VMEM((4, row_count, piece), bf16),
-            pltpu.VMEM((3, experts, 8, piece), bf16),
-            pltpu.VMEM((3, experts, 8, piece), bf16),
-            pltpu.VMEM((4, 2, tokens, 8 * experts), bf16),
-            dma((3,)),
-            dma((3,)),
-            dma((3,)),
-            dma((3,)),
-            dma((3,)),
-            dma((3,)),
-            dma((3,)),
-            dma((4,)),
-            dma((4,)),
-            dma((3,)),
-            dma((3,)),
-            dma((3,)),
-        ],
-        compiler_params=pltpu.CompilerParams(
-            collective_id=0, has_side_effects=True, vmem_limit_bytes=VMEM_LIMIT
-        ),
-        name="experts",
-    )(
-        expert_input,
-        expert_gain.reshape(1, width),
-        routes.T.reshape(1, -1),
-        route_weight.T,
-        expert_gate[0],
-        expert_up[0],
-        expert_down[0],
-    )
+    wait_bytes(state_send.at[pl.ds(0, slab - 1)], state_sems.at[0])
+    wait_bytes(slab_got.at[pl.ds(0, nz - 1)], state_sems.at[2])
+    wait_bytes(enter_send.at[pl.ds(0, slab - 1)], state_sems.at[4])
 
 
 def on_device(
@@ -552,21 +642,110 @@
     expert_up,
     expert_down,
 ):
-    mixer_output = mixer_half(
+    tokens, width = expert_input.shape
+    experts = lax.axis_size(EP)
+    slab, slabs = lax.axis_size("ep_1") * lax.axis_size("ep_2"), lax.axis_size("ep_0")
+    shard = expert_gate.shape[2]
+    piece = width // 4
+    row_count = experts * CAP
+    mix_rows, heads = log_decay.shape
+    mix_width = heads * HEAD
+    block_count = mix_rows // BLOCK
+    share = HEAD // slab
+    unit = mix_rows // 4
+    bf16, f32 = jnp.bfloat16, jnp.float32
+
+    half_dim = HEAD // 2
+    position = lax.axis_index(EP) * mix_rows + jnp.arange(mix_rows, dtype=jnp.int32)
+    frequency = 10000.0 ** (-jnp.arange(half_dim, dtype=f32) / half_dim)
+    angles = position.astype(f32)[:, None] * frequency[None, :]
+    cosine, sine = jnp.cos(angles), jnp.sin(angles)
+    cosine = jnp.concatenate([cosine, cosine], axis=1)
+    sine = jnp.concatenate([-sine, sine], axis=1)
+    log_rows = log_decay.T.reshape(heads, block_count, BLOCK).transpose(1, 0, 2)
+
+    vmem = pl.BlockSpec(memory_space=pltpu.VMEM)
+    anywhere = pl.BlockSpec(memory_space=pl.ANY)
+    dma = pltpu.SemaphoreType.DMA
+    return pl.pallas_call(
+        layer_kernel,
+        out_shape=(
+            jax.ShapeDtypeStruct((unit, width), bf16),
+            jax.ShapeDtypeStruct((tokens, width), bf16),
+        ),
+        in_specs=[vmem] * 4
+        + [anywhere] * 4
+        + [vmem]
+        + [anywhere] * 4
+        + [vmem, anywhere]
+        + [vmem] * 4,
+        out_specs=(vmem, vmem),
+        scratch_shapes=[
+            pltpu.VMEM((3, experts, 8, piece), bf16),
+            pltpu.VMEM((2, 3, experts, 8, piece), bf16),
+            pltpu.VMEM((2, row_count, width), bf16),
+            pltpu.VMEM((2, width, shard), bf16),
+            pltpu.VMEM((2, width, shard), bf16),
+            pltpu.VMEM((2, shard, width), bf16),
+            pltpu.VMEM((2, 2, row_count, shard), bf16),
+            pltpu.VMEM((4, row_count, piece), bf16),
+            pltpu.VMEM((4, row_count, piece), bf16),
+            pltpu.VMEM((3, experts, 8, piece), bf16),
+            pltpu.VMEM((3, experts, 8, piece), bf16),
+            pltpu.VMEM((4, 2, tokens, 8 * experts), bf16),
+        ]
+        + [dma((3,))] * 7
+        + [dma((4,))] * 2
+        + [dma((3,))] * 3
+        + [
+            pltpu.VMEM((mix_rows, width), bf16),
+            pltpu.VMEM((4, width, mix_width), bf16),
+            pltpu.VMEM((mix_width, width), bf16),
+            pltpu.VMEM((mix_rows, mix_width), bf16),
+            pltpu.VMEM((mix_rows, mix_width), bf16),
+            pltpu.VMEM((mix_rows, mix_width), bf16),
+            pltpu.VMEM((mix_rows, mix_width), bf16),
+            pltpu.VMEM((mix_rows, mix_width), f32),
+            pltpu.VMEM((block_count, heads, HEAD, HEAD), f32),
+            pltpu.VMEM((block_count, heads, 8, HEAD), f32),
+            pltpu.VMEM((mix_rows, width), bf16),
+            pltpu.VMEM((slab, heads, share + 8, HEAD), f32),
+            pltpu.VMEM((slab, heads, share + 8, HEAD), f32),
+            pltpu.VMEM((heads, share + 8, HEAD), f32),
+            pltpu.VMEM((slabs, heads, share + 8, HEAD), f32),
+            pltpu.VMEM((slab, heads, share, HEAD), f32),
+            pltpu.VMEM((slab, heads, share, HEAD), f32),
+            pltpu.VMEM((2, unit, width // 2), bf16),
+            pltpu.VMEM((2, unit, width), bf16),
+            dma((6,)),
+            dma((6,)),
+        ]
+        + [dma((2,))] * 6,
+        compiler_params=pltpu.CompilerParams(
+            collective_id=0, has_side_effects=True, vmem_limit_bytes=VMEM_LIMIT
+        ),
+        name="layer",
+    )(
+        expert_input,
+        expert_gain.reshape(1, width),
+        routes.T.reshape(1, -1),
+        route_weight.T,
+        expert_gate[0],
+        expert_up[0],
+        expert_down[0],
         mixer_input,
-        mixer_gain,
+        mixer_gain.reshape(1, width),
         query_weight,
         key_weight,
         value_weight,
         gate_weight,
-        head_gain,
+        head_gain.reshape(1, mix_width),
         output_weight,
         log_decay,
-    )
-    expert_output = expert_half(
-        expert_input, expert_gain, routes, route_weight, expert_gate, expert_up, expert_down
-    )
-    return (mixer_output, expert_output)
+        log_rows,
+        cosine,
+        sine,
+    )
 
 
 def solution(mesh):

time: 245 us -> 138 us (0.56)
  blocking collectives: 68.2 us -> 0 us
  matrix products: 15.4 us -> 0 us
  between operations: 15.1 us -> 0.67 us
  local copies, waits for them, and re-layouts: 11 us -> 5.3 us
  other arithmetic: 4.48 us -> 2 us
    all_gather x5 -> x0, blocking collectives: 65.8 us -> none  [carried_in(): lax.all_gather(part.astype(kind), axis)]
    dot_general x8 -> x0, matrix products: 15.4 us -> none  [the longest x1 5.59 us: mixer_half(): jnp.dot(mixer_hidden, output_weight, preferred_element_type=jnp.float32)]
    unnamed x18 -> x3, local copies, waits for them, and re-layouts: 3.44 us -> 5.3 us
  transfers between devices with their start and end apart: 1 -> 0, of which waited for: 0 -> 0; matrix products, arithmetic and copies ran while one was open for 0% -> 0% of each run, Pallas kernels for 53% -> 0%
where the time goes in v2:
time: 138 us; the launch traced here: 135 us
  Pallas kernels  127 us (92%)
  local copies, waits for them, and re-layouts  5.3 us (4%)
  other arithmetic  2 us (1%)
    pallas_call x1, Pallas kernels, on_device(): pl.pallas_call(layer_kernel, out_shape=(jax.ShapeDtypeStruct((unit, width...  127 us
    unnamed x3, local copies, waits for them, and re-layouts  5.3 us

profile of v2, /device:TPU:2, one launch (start us, length us, event | category | flops | bytes accessed | tf_op | source)
XLA Modules:
  0.0 135.4 jit_solution(2845642186572630066)
XLA Ops:
  0.7 1.5 %copy.18.logs_ref = f32[512,2]{1,0:T(8,128)} copy(f32[512,2]{0,1:T(2,128)} %param.24) | data formatting | bytes 8192 | tf_op args[8]
  2.2 1.0 fusion
  3.2 1.0 pad_maximum_fusion
  4.2 127.5 %layer.1 = (bf16[128,2048]{1,0:T(8,128)(2,1)}, bf16[128,2048]{1,0:T(8,128)(2,1)}) custom-call(bf16[128,2048]{1,0:T(8,128)(2,1)} %x_ref.1, f32[1,2048]{1,0:T(1,128)} %bitcast.19, s32[1,256]{1,0:T(1,128)} %bitcast.21, f32[2,128]{1,0:T(2,128)} %bitcast.22, bf16[2048,256]{1,0:T(8,128)(2,1)} %bitcast.15, bf16[2048,256]{1,0:T(8,128)(2,1)} %bitcast.16, ...), custom_call_target="tpu_custom_call" | custom-call | tf_op jit(solution)/shard_map/layer/pallas_call | solution.py:670
  131.7 1.9 %copy.21 = bf16[128,2048]{1,0:T(8,128)(2,1)} copy(bf16[128,2048]{1,0:T(8,128)(2,1)} %get-tuple-element.9) | data formatting | bytes 1048576
  133.6 1.9 %copy.22 = bf16[128,2048]{1,0:T(8,128)(2,1)} copy(bf16[128,2048]{1,0:T(8,128)(2,1)} %get-tuple-element.10) | data formatting | bytes 1048576
  (2 shorter events, 0.0 us)

commit v3 on v2

--- a/solution.py
+++ b/solution.py
@@ -13,9 +13,11 @@
 EP_TP = ("ep_0", "ep_1", "ep_2", "tp")
 EPS = 1e-06
 CAP = 6
+CHUNKS = (1, 1, 1, 1, 1, 1)
 HEAD = 128
+FINE = 64
 MESH_ID = pl.DeviceIdType.MESH
-VMEM_LIMIT = 64 * 1024 * 1024 - 1024 * 1024
+VMEM_LIMIT = 66060288
 
 
 def z_order(count):
@@ -68,13 +70,14 @@
     pltpu.make_async_copy(ref, ref, sem).wait()
 
 
-def packed_ids(shape, dim, piece):
+def folded_rows(shape, dim, group, count):
+    fold = 8 // count
     row = lax.broadcasted_iota(jnp.int32, shape, dim)
-    owner = (row // 8) * CAP
-    lane = row % 8
-    if piece is None:
-        return jnp.where(lane < CAP, owner + lane, -1)
-    return jnp.where(lane == 6, owner + piece, jnp.where(lane == 7, owner + 3 + piece, -1))
+    return ((row % fold) * count + (row % 8) // fold) * group + row // 8
+
+
+def flag(condition):
+    return jnp.where(condition, 1.0, 0.0).astype(jnp.bfloat16)
 
 
 def dot(a, b):
@@ -95,7 +98,14 @@
         floats = mx_buf[span, :].astype(jnp.float32)
         scale = lax.rsqrt(jnp.mean(floats * floats, axis=-1, keepdims=True) + EPS)
         normed = (floats * scale * mx_gain[...]).astype(jnp.bfloat16)
-        cosine, sine = cos_ref[span, :], sin_ref[span, :]
+        cosines, sines = [], []
+        for a in range(step_rows // FINE):
+            base_cos = cos_ref[pl.ds(FINE + i * (step_rows // FINE) + a, 1), :]
+            base_sin = sin_ref[pl.ds(FINE + i * (step_rows // FINE) + a, 1), :]
+            fine_cos, fine_sin = cos_ref[:FINE, :], sin_ref[:FINE, :]
+            cosines.append(base_cos * fine_cos - base_sin * fine_sin)
+            sines.append(base_sin * fine_cos + base_cos * fine_sin)
+        cosine, sine = jnp.concatenate(cosines, axis=0), jnp.concatenate(sines, axis=0)
         for n, target in enumerate((q_buf, k_buf, v_buf, g_buf)):
             raw = dot(normed, mixer_weights[n]).astype(jnp.bfloat16)
             if n >= 2:
@@ -113,20 +123,20 @@
     lax.fori_loop(0, row_count // step_rows, step, 0)
 
 
-def scan_blocks(logs_ref, log_rows_ref, q_buf, k_buf, v_buf, inner_buf, update_buf, decay_buf):
+def scan_blocks(log_rows_ref, q_buf, k_buf, v_buf, inner_buf, update_buf, decay_buf):
     block_count = q_buf.shape[0] // BLOCK
     heads = q_buf.shape[1] // HEAD
     row_ids = lax.broadcasted_iota(jnp.int32, (BLOCK, BLOCK), 0)
     col_ids = lax.broadcasted_iota(jnp.int32, (BLOCK, BLOCK), 1)
-    lower, upper = col_ids <= row_ids, row_ids <= col_ids
+    lower = col_ids <= row_ids
 
     def step(b, carry):
         span = pl.ds(pl.multiple_of(b * BLOCK, BLOCK), BLOCK)
-        tall, wide = logs_ref[span, :], log_rows_ref[b]
+        wide = log_rows_ref[b]
         for h in range(heads):
             lanes = slice(h * HEAD, (h + 1) * HEAD)
             cum_col = jnp.sum(jnp.where(lower, wide[h : h + 1, :], 0.0), axis=1, keepdims=True)
-            cum_row = jnp.sum(jnp.where(upper, tall[:, h : h + 1], 0.0), axis=0, keepdims=True)
+            cum_row = jnp.broadcast_to(cum_col, (BLOCK, BLOCK)).T
             total = jnp.sum(wide[h : h + 1, :], axis=1, keepdims=True)
             q, k, v = q_buf[span, lanes], k_buf[span, lanes], v_buf[span, lanes]
             scaled = (k.astype(jnp.float32) * jnp.exp(total - cum_col)).astype(jnp.bfloat16)
@@ -189,24 +199,26 @@
     g_hbm,
     head_gain,
     o_hbm,
-    logs_ref,
     log_rows_ref,
     cos_ref,
     sin_ref,
     mixed_ref,
     out_ref,
+    picked,
     send_buf,
     arrived,
+    passed,
     rows,
     gate_buf,
     up_buf,
     down_buf,
-    hidden,
     part_send,
     part_recv,
     back_send,
     back,
     weigh,
+    result_rows,
+    total_buf,
     dispatch_send,
     dispatch_recv,
     forward_send,
@@ -255,8 +267,6 @@
     token_peer = {"tp": (1 - c) * mirror + c * flip}
     experts = nz * nx * nc
     tokens, width = x_ref.shape
-    piece = width // 4
-    row_count = experts * CAP
     group = min(32, experts)
     group_count = experts // group
 
@@ -267,6 +277,12 @@
         loads.append(pltpu.make_async_copy(source, mixer_weights.at[n], load_sem.at[1 + n]))
     loads.append(pltpu.make_async_copy(o_hbm, o_buf, load_sem.at[5]))
 
+    locals_ = []
+    for k, (source, target) in enumerate(
+        ((gate_hbm, gate_buf), (up_hbm, up_buf), (down_hbm, down_buf))
+    ):
+        locals_.append(pltpu.make_async_copy(source, target.at[0], weight_local.at[k]))
+
     barrier = pltpu.get_barrier_semaphore()
     for_each_peer(
         lambda device, index: pl.semaphore_signal(
@@ -275,16 +291,98 @@
     )
     for peer in (weight_peer, token_peer):
         pl.semaphore_signal(barrier, inc=1, device_id=peer, device_id_type=MESH_ID)
-    locals_ = []
-    for k, (source, target) in enumerate(
-        ((gate_hbm, gate_buf), (up_hbm, up_buf), (down_hbm, down_buf))
-    ):
-        locals_.append(pltpu.make_async_copy(source, target.at[0], weight_local.at[k]))
-        locals_[-1].start()
-    for load in loads:
+    for load in loads + locals_:
         load.start()
+
+    floats = x_ref[...].astype(jnp.float32)
+    scale = lax.rsqrt(jnp.mean(floats * floats, axis=-1, keepdims=True) + EPS)
+    normed = (floats * scale * gain_ref[...]).astype(jnp.bfloat16)
+
+    entries = 2 * tokens
+    routes = routes_ref[...]
+    named = lax.broadcasted_iota(jnp.int32, (experts, entries), 0) == routes
+    named_bf = jnp.where(named, 1.0, 0.0).astype(jnp.bfloat16)
+    earlier = lax.broadcasted_iota(jnp.int32, (entries, entries), 0) < lax.broadcasted_iota(
+        jnp.int32, (entries, entries), 1
+    )
+    prior = dot(named_bf, jnp.where(earlier, 1.0, 0.0).astype(jnp.bfloat16))
+    slot = jnp.sum(jnp.where(named, prior, 0.0), axis=0, keepdims=True).astype(jnp.int32)
+    target = routes * CAP + slot
+    first, second = target[:, :tokens], target[:, tokens:]
+    scores = score_ref[...]
+    shares = scores / jnp.sum(scores, axis=0, keepdims=True)
+
+    places = (experts, tokens)
+    firsts = [0]
+    for count in CHUNKS:
+        firsts.append(firsts[-1] + count)
+
+    def slot_ids(n):
+        return lax.broadcasted_iota(jnp.int32, places, 0) * CAP + n
+
+    chosen = jnp.concatenate(
+        [flag((slot_ids(n) == first) | (slot_ids(n) == second)) for n in range(CAP)], axis=0
+    )
+    picked[...] = dot(chosen, normed).astype(jnp.bfloat16)
+
+    block = 8 * group
+    spreads, gathers = {}, {}
+    for count in sorted(set(CHUNKS)):
+        square = (block, block)
+        spreads[count] = flag(
+            folded_rows(square, 1, group, count) == lax.broadcasted_iota(jnp.int32, square, 0)
+        )
+        gathers[count] = flag(
+            folded_rows(square, 0, group, count) == lax.broadcasted_iota(jnp.int32, square, 1)
+        )
+
+    def spans(p):
+        count = CHUNKS[p]
+        piece = width * count // 8
+        for q in range(8 // count):
+            for r in range(count):
+                yield r, slice(q * piece, (q + 1) * piece)
+
+    def fold(p, source, base, target):
+        count = CHUNKS[p]
+        for g in range(group_count):
+            lined = jnp.concatenate(
+                [
+                    source[base + r * experts + g * group : base + r * experts + (g + 1) * group, columns]
+                    for r, columns in spans(p)
+                ],
+                axis=0,
+            )
+            target[p][g * group : (g + 1) * group] = (
+                dot(gathers[count], lined).astype(jnp.bfloat16).reshape(group, 8, -1)
+            )
+
+    def unfold(p, source, store):
+        count = CHUNKS[p]
+        whole = source[...].reshape(8 * experts, -1)
+        for g in range(group_count):
+            lined = dot(spreads[count], whole[g * block : (g + 1) * block]).astype(jnp.bfloat16)
+            for n, (r, columns) in enumerate(spans(p)):
+                low = r * experts + g * group
+                store(slice(low, low + group), columns, lined[n * group : (n + 1) * group])
+
+    def exchange(p, source, target, send_sem, recv_sem):
+        for_each_peer(
+            lambda device, index: remote(
+                source[p].at[index], target[p].at[me], send_sem.at[p], recv_sem.at[p], device
+            ).start()
+        )
+        pltpu.make_async_copy(source[p].at[me], target[p].at[me], own_sem.at[p]).start()
+
+    def exchanged(p, source, target, recv_sem):
+        wait_bytes(source[p].at[pl.ds(0, experts - 1)], recv_sem.at[p])
+        pltpu.make_async_copy(source[p].at[me], target[p].at[me], own_sem.at[p]).wait()
+
+    chunks = range(len(CHUNKS))
+    for p in chunks:
+        fold(p, picked, firsts[p] * experts, send_buf)
+
     pl.semaphore_wait(barrier, experts + 1)
-
     weights_out = [
         remote(gate_hbm, gate_buf.at[1], weight_send.at[0], weight_recv.at[0], weight_peer),
         remote(up_hbm, up_buf.at[1], weight_send.at[1], weight_recv.at[1], weight_peer),
@@ -292,50 +390,13 @@
     ]
     for copy in weights_out:
         copy.start()
-
-    floats = x_ref[...].astype(jnp.float32)
-    scale = lax.rsqrt(jnp.mean(floats * floats, axis=-1, keepdims=True) + EPS)
-    normed = (floats * scale * gain_ref[...]).astype(jnp.bfloat16)
-
-    entries = 2 * tokens
-    routes = routes_ref[...]
-    named = lax.broadcasted_iota(jnp.int32, (experts, entries), 0) == routes
-    named_bf = jnp.where(named, 1.0, 0.0).astype(jnp.bfloat16)
-    earlier = lax.broadcasted_iota(jnp.int32, (entries, entries), 0) < lax.broadcasted_iota(
-        jnp.int32, (entries, entries), 1
-    )
-    prior = dot(named_bf, jnp.where(earlier, 1.0, 0.0).astype(jnp.bfloat16))
-    slot = jnp.sum(jnp.where(named, prior, 0.0), axis=0, keepdims=True).astype(jnp.int32)
-    target = routes * CAP + slot
-    first, second = target[:, :tokens], target[:, tokens:]
-    scores = score_ref[...]
-    shares = scores / jnp.sum(scores, axis=0, keepdims=True)
-
-    packed = (8 * experts, tokens)
-    ids = [packed_ids(packed, 0, j) for j in (None, 0, 1, 2)]
-    picks = [
-        jnp.where((i == first) | (i == second), 1.0, 0.0).astype(jnp.bfloat16) for i in ids
-    ]
-    last = normed[:, 3 * piece :]
-    for j in range(3):
-        chosen = jnp.concatenate([picks[0], picks[1 + j]], axis=1)
-        source = jnp.concatenate([normed[:, j * piece : (j + 1) * piece], last], axis=0)
-        send_buf[j] = dot(chosen, source).astype(jnp.bfloat16).reshape(experts, 8, piece)
-        for_each_peer(
-            lambda device, index, j=j: remote(
-                send_buf.at[j, index],
-                arrived.at[0, j, me],
-                dispatch_send.at[j],
-                dispatch_recv.at[j],
-                device,
-            ).start()
-        )
-        pltpu.make_async_copy(send_buf.at[j, me], arrived.at[0, j, me], own_sem.at[j]).start()
+    for p in chunks:
+        exchange(p, send_buf, arrived, dispatch_send, dispatch_recv)
 
     for load in loads:
         load.wait()
     project_rows(mx_buf, mx_gain, mixer_weights, cos_ref, sin_ref, q_buf, k_buf, v_buf, g_buf)
-    scan_blocks(logs_ref, log_rows_ref, q_buf, k_buf, v_buf, inner_buf, update_buf, decay_buf)
+    scan_blocks(log_rows_ref, q_buf, k_buf, v_buf, inner_buf, update_buf, decay_buf)
     block_count, heads = update_buf.shape[:2]
     share = HEAD // slab
     for h in range(heads):
@@ -363,41 +424,82 @@
     )
     state_got[spot] = state_send[spot]
 
-    for n, i in enumerate(ids):
-        shared = jnp.where(i == first, shares[0:1], 0.0) + jnp.where(
-            i == second, shares[1:2], 0.0
+    for p in chunks:
+        turned = jnp.concatenate(
+            [
+                jnp.where(slot_ids(n) == first, shares[0:1], 0.0)
+                + jnp.where(slot_ids(n) == second, shares[1:2], 0.0)
+                for n in range(firsts[p], firsts[p + 1])
+            ],
+            axis=0,
+        ).T
+        high = turned.astype(jnp.bfloat16)
+        weigh[p][:tokens] = high
+        weigh[p][tokens:] = (turned - high.astype(jnp.float32)).astype(jnp.bfloat16)
+
+    def unpack(side, p, source):
+        def store(low, columns, value):
+            rows[p][side, low, columns] = value
+
+        unfold(p, source[p], store)
+
+    forwards, parts, hiddens = {}, {}, {}
+
+    def forward(p):
+        exchanged(p, send_buf, arrived, dispatch_recv)
+        forwards[p] = remote(
+            arrived[p], passed[p], forward_send.at[p], forward_recv.at[p], token_peer
         )
-        turned = shared.T
-        high = turned.astype(jnp.bfloat16)
-        weigh[n, 0] = high
-        weigh[n, 1] = (turned - high.astype(jnp.float32)).astype(jnp.bfloat16)
-
-    shape = (group * CAP, group * 8)
-    spread = [
-        jnp.where(
-            packed_ids(shape, 1, j) == lax.broadcasted_iota(jnp.int32, shape, 0), 1.0, 0.0
-        ).astype(jnp.bfloat16)
-        for j in (None, 0, 1, 2)
-    ]
-    spread_last = jnp.concatenate(spread[1:], axis=1)
-
-    def unpack(side, j):
-        block = arrived[side, j].reshape(8 * experts, piece)
-        for g in range(group_count):
-            rows[side, g * group * CAP : (g + 1) * group * CAP, j * piece : (j + 1) * piece] = dot(
-                spread[0], block[g * group * 8 : (g + 1) * group * 8]
-            ).astype(jnp.bfloat16)
-
-    def unpack_last(side):
-        blocks = [arrived[side, j].reshape(8 * experts, piece) for j in range(3)]
-        for g in range(group_count):
-            stacked = jnp.concatenate(
-                [block[g * group * 8 : (g + 1) * group * 8] for block in blocks], axis=0
+        forwards[p].start()
+        unpack(0, p, arrived)
+
+    def contract(hidden):
+        return dot(hidden, down_buf[...].reshape(-1, width))
+
+    def compute(p):
+        forwards[p].wait_recv()
+        unpack(1, p, passed)
+        own_rows = CHUNKS[p] * experts
+        source = rows[p][...].reshape(2 * own_rows, width)
+        halves = []
+        for half in range(2):
+            gate_part = dot(source, gate_buf[half])
+            up_part = dot(source, up_buf[half])
+            halves.append(
+                (gate_part / (1.0 + jnp.exp(-gate_part)) * up_part).astype(jnp.bfloat16)
             )
-            rows[side, g * group * CAP : (g + 1) * group * CAP, 3 * piece :] = dot(
-                spread_last, stacked
-            ).astype(jnp.bfloat16)
-
+        hidden = jnp.concatenate(halves, axis=1)
+        part_send[p][...] = contract(hidden[own_rows:]).astype(jnp.bfloat16)
+        parts[p] = remote(
+            part_send[p], part_recv[p], part_send_sem.at[p], part_recv_sem.at[p], token_peer
+        )
+        parts[p].start()
+        hiddens[p] = hidden[:own_rows]
+
+    def give_back(p):
+        own = contract(hiddens[p])
+        parts[p].wait_recv()
+        result = (own + part_recv[p][...].astype(jnp.float32)).astype(jnp.bfloat16)
+        fold(p, result, 0, back_send)
+        exchange(p, back_send, back, back_send_sem, back_recv_sem)
+
+    def combine(p):
+        exchanged(p, back_send, back, back_recv_sem)
+
+        def store(low, columns, value):
+            result_rows[p][low, columns] = value
+
+        unfold(p, back[p], store)
+        sums = dot(weigh[p][...], result_rows[p][...])
+        part = sums[:tokens] + sums[tokens:]
+        if p > 0:
+            part = part + total_buf[...]
+        if p < len(CHUNKS) - 1:
+            total_buf[...] = part
+        else:
+            out_ref[...] = part.astype(jnp.bfloat16)
+
+    forward(0)
     wait_bytes(state_send.at[pl.ds(0, slab - 1)], state_sems.at[1])
     running = [jnp.zeros((share, HEAD), jnp.float32)] * heads
     decayed = [jnp.zeros((1, HEAD), jnp.float32)] * heads
@@ -426,24 +528,14 @@
     lax.fori_loop(1, nz, z_step, 0)
     slab_got[z] = slab_send[...]
 
-    forwards = []
-
-    def forward(j):
-        wait_bytes(send_buf.at[j, pl.ds(0, experts - 1)], dispatch_recv.at[j])
-        pltpu.make_async_copy(send_buf.at[j, me], arrived.at[0, j, me], own_sem.at[j]).wait()
-        forwards.append(
-            remote(
-                arrived.at[0, j],
-                arrived.at[1, j],
-                forward_send.at[j],
-                forward_recv.at[j],
-                token_peer,
-            )
-        )
-        forwards[-1].start()
-        unpack(0, j)
-
-    forward(0)
+    forward(1)
+    for k in range(2):
+        locals_[k].wait()
+        weights_out[k].wait_recv()
+    locals_[2].wait()
+    weights_out[2].wait_recv()
+    compute(0)
+    forward(2)
     wait_bytes(slab_got.at[pl.ds(0, nz - 1)], state_sems.at[3])
     for h in range(heads):
         entry = jnp.zeros((share, HEAD), jnp.float32)
@@ -461,53 +553,25 @@
         ).start()
     )
     enter_got[spot] = enter_send[spot]
+    compute(1)
+    give_back(0)
+    forward(3)
+    compute(2)
     wait_bytes(enter_send.at[pl.ds(0, slab - 1)], state_sems.at[5])
     entering = [
         jnp.concatenate([enter_got[n, h] for n in range(slab)], axis=0) for h in range(heads)
     ]
-    forward(1)
+    give_back(1)
+    forward(4)
     finish_blocks(
         entering, q_buf, g_buf, inner_buf, update_buf, decay_buf, head_gain, o_buf, mix_buf
     )
-    forward(2)
-    unpack_last(0)
-
-    def expand(side, half):
-        source = rows[side]
-        gate_part = dot(source, gate_buf[half])
-        up_part = dot(source, up_buf[half])
-        hidden[side, half] = (gate_part / (1.0 + jnp.exp(-gate_part)) * up_part).astype(
-            jnp.bfloat16
-        )
-
-    locals_[0].wait()
-    locals_[1].wait()
-    expand(0, 0)
-    for j in range(3):
-        forwards[j].wait_recv()
-        unpack(1, j)
-    unpack_last(1)
-    expand(1, 0)
-    weights_out[0].wait_recv()
-    weights_out[1].wait_recv()
-    expand(1, 1)
-
-    def contract(side, k):
-        columns = slice(k * piece, (k + 1) * piece)
-        return dot(hidden[side, 0], down_buf[0, :, columns]) + dot(
-            hidden[side, 1], down_buf[1, :, columns]
-        )
-
-    locals_[2].wait()
-    weights_out[2].wait_recv()
-    parts = {}
-    for k in (3, 0, 1, 2):
-        part_send[k] = contract(1, k).astype(jnp.bfloat16)
-        parts[k] = remote(
-            part_send.at[k], part_recv.at[k], part_send_sem.at[k], part_recv_sem.at[k], token_peer
-        )
-        parts[k].start()
-
+    compute(3)
+    give_back(2)
+    forward(5)
+    compute(4)
+    give_back(3)
+    compute(5)
     unit = mix_buf.shape[0] // 4
     half = width // 2
     right, left = lax.rem(y + 1, 4), lax.rem(y + 3, 4)
@@ -539,43 +603,8 @@
         )
     for copy in directs:
         copy.start()
-    expand(0, 1)
-
-    def total(k):
-        own = contract(0, k)
-        parts[k].wait_recv()
-        return (own + part_recv[k].astype(jnp.float32)).astype(jnp.bfloat16)
-
-    gather = [
-        jnp.where(
-            packed_ids((group * 8, group * CAP), 0, j)
-            == lax.broadcasted_iota(jnp.int32, (group * 8, group * CAP), 1),
-            1.0,
-            0.0,
-        ).astype(jnp.bfloat16)
-        for j in (None, 0, 1, 2)
-    ]
-    tail = total(3)
-    for j in range(3):
-        body = total(j)
-        for g in range(group_count):
-            span = slice(g * group * CAP, (g + 1) * group * CAP)
-            back_send[j, g * group : (g + 1) * group] = (
-                (dot(gather[0], body[span]) + dot(gather[1 + j], tail[span]))
-                .astype(jnp.bfloat16)
-                .reshape(group, 8, piece)
-            )
-        for_each_peer(
-            lambda device, index, j=j: remote(
-                back_send.at[j, index],
-                back.at[j, me],
-                back_send_sem.at[j],
-                back_recv_sem.at[j],
-                device,
-            ).start()
-        )
-        pltpu.make_async_copy(back_send.at[j, me], back.at[j, me], own_sem.at[j]).start()
-
+    give_back(4)
+    give_back(5)
     summed = []
     for n, (peer, relayed, plain) in enumerate(sides):
         directs[2 * n].wait_recv()
@@ -592,6 +621,10 @@
             )
         )
         summed[-1].start()
+    combine(0)
+    combine(1)
+    combine(2)
+    combine(3)
     for n in range(2):
         directs[2 * n + 1].wait_recv()
         summed[n].wait_recv()
@@ -601,24 +634,15 @@
         + side_got[1].astype(jnp.float32)
     ).astype(jnp.bfloat16)
 
-    rest = jnp.zeros((tokens, piece), jnp.float32)
-    for j in range(3):
-        wait_bytes(back_send.at[j, pl.ds(0, experts - 1)], back_recv_sem.at[j])
-        pltpu.make_async_copy(back_send.at[j, me], back.at[j, me], own_sem.at[j]).wait()
-        block = back[j].reshape(8 * experts, piece)
-        out_ref[:, j * piece : (j + 1) * piece] = (
-            dot(weigh[0, 0], block) + dot(weigh[0, 1], block)
-        ).astype(jnp.bfloat16)
-        rest = rest + dot(weigh[1 + j, 0], block) + dot(weigh[1 + j, 1], block)
-    out_ref[:, 3 * piece :] = rest.astype(jnp.bfloat16)
-
-    for copy in weights_out + forwards + list(parts.values()) + directs + summed:
+    combine(4)
+    combine(5)
+    for copy in (
+        weights_out + list(forwards.values()) + list(parts.values()) + directs + summed
+    ):
         copy.wait_send()
-    for j in range(3):
-        wait_bytes(send_buf.at[j, pl.ds(0, experts - 1)], dispatch_send.at[j])
-        wait_bytes(back_send.at[j, pl.ds(0, experts - 1)], back_send_sem.at[j])
-
-
+    for p in chunks:
+        wait_bytes(send_buf[p].at[pl.ds(0, experts - 1)], dispatch_send.at[p])
+        wait_bytes(back_send[p].at[pl.ds(0, experts - 1)], back_send_sem.at[p])
     wait_bytes(state_send.at[pl.ds(0, slab - 1)], state_sems.at[0])
     wait_bytes(slab_got.at[pl.ds(0, nz - 1)], state_sems.at[2])
     wait_bytes(enter_send.at[pl.ds(0, slab - 1)], state_sems.at[4])
@@ -646,8 +670,10 @@
     experts = lax.axis_size(EP)
     slab, slabs = lax.axis_size("ep_1") * lax.axis_size("ep_2"), lax.axis_size("ep_0")
     shard = expert_gate.shape[2]
-    piece = width // 4
-    row_count = experts * CAP
+    messages = [
+        pltpu.VMEM((experts, 8, width * count // 8), jnp.bfloat16) for count in CHUNKS
+    ]
+    chunk_rows = [pltpu.VMEM((count * experts, width), jnp.bfloat16) for count in CHUNKS]
     mix_rows, heads = log_decay.shape
     mix_width = heads * HEAD
     block_count = mix_rows // BLOCK
@@ -656,17 +682,20 @@
     bf16, f32 = jnp.bfloat16, jnp.float32
 
     half_dim = HEAD // 2
-    position = lax.axis_index(EP) * mix_rows + jnp.arange(mix_rows, dtype=jnp.int32)
-    frequency = 10000.0 ** (-jnp.arange(half_dim, dtype=f32) / half_dim)
+    lane = jnp.arange(HEAD, dtype=jnp.int32)
+    frequency = 10000.0 ** (-(lane % half_dim).astype(f32) / half_dim)
+    row = jnp.arange(FINE + mix_rows // FINE, dtype=jnp.int32)
+    coarse = lax.axis_index(EP) * mix_rows + (row - FINE) * FINE
+    position = jnp.where(row < FINE, row, coarse)
     angles = position.astype(f32)[:, None] * frequency[None, :]
-    cosine, sine = jnp.cos(angles), jnp.sin(angles)
-    cosine = jnp.concatenate([cosine, cosine], axis=1)
-    sine = jnp.concatenate([-sine, sine], axis=1)
+    cosine = jnp.cos(angles)
+    sine = jnp.where(lane < half_dim, -1.0, 1.0) * jnp.sin(angles)
     log_rows = log_decay.T.reshape(heads, block_count, BLOCK).transpose(1, 0, 2)
 
     vmem = pl.BlockSpec(memory_space=pltpu.VMEM)
-    anywhere = pl.BlockSpec(memory_space=pl.ANY)
+    anywhere = pl.BlockSpec(memory_space=pltpu.HBM)
     dma = pltpu.SemaphoreType.DMA
+    chunk_sems = dma((len(CHUNKS),))
     return pl.pallas_call(
         layer_kernel,
         out_shape=(
@@ -678,25 +707,28 @@
         + [vmem]
         + [anywhere] * 4
         + [vmem, anywhere]
-        + [vmem] * 4,
+        + [vmem] * 3,
         out_specs=(vmem, vmem),
         scratch_shapes=[
-            pltpu.VMEM((3, experts, 8, piece), bf16),
-            pltpu.VMEM((2, 3, experts, 8, piece), bf16),
-            pltpu.VMEM((2, row_count, width), bf16),
+            pltpu.VMEM((CAP * experts, width), bf16),
+            messages,
+            messages,
+            messages,
+            [pltpu.VMEM((2, count * experts, width), bf16) for count in CHUNKS],
             pltpu.VMEM((2, width, shard), bf16),
             pltpu.VMEM((2, width, shard), bf16),
             pltpu.VMEM((2, shard, width), bf16),
-            pltpu.VMEM((2, 2, row_count, shard), bf16),
-            pltpu.VMEM((4, row_count, piece), bf16),
-            pltpu.VMEM((4, row_count, piece), bf16),
-            pltpu.VMEM((3, experts, 8, piece), bf16),
-            pltpu.VMEM((3, experts, 8, piece), bf16),
-            pltpu.VMEM((4, 2, tokens, 8 * experts), bf16),
+            chunk_rows,
+            chunk_rows,
+            messages,
+            messages,
+            [pltpu.VMEM((2 * tokens, count * experts), bf16) for count in CHUNKS],
+            chunk_rows,
+            pltpu.VMEM((tokens, width), f32),
         ]
-        + [dma((3,))] * 7
-        + [dma((4,))] * 2
+        + [chunk_sems] * 4
         + [dma((3,))] * 3
+        + [chunk_sems] * 5
         + [
             pltpu.VMEM((mix_rows, width), bf16),
             pltpu.VMEM((4, width, mix_width), bf16),
@@ -741,7 +773,6 @@
         gate_weight,
         head_gain.reshape(1, mix_width),
         output_weight,
-        log_decay,
         log_rows,
         cosine,
         sine,

time: 138 us -> 111 us (0.80); the launches traced: 135 us -> 111 us
  Pallas kernels: 127 us -> 106 us
  local copies, waits for them, and re-layouts: 5.3 us -> 3.76 us
    pallas_call x1, Pallas kernels: 127 us -> 106 us  [on_device(): pl.pallas_call(layer_kernel, out_shape=(jax.ShapeDtypeStruct((unit, width...]
    unnamed x3 -> x2, local copies, waits for them, and re-layouts: 5.3 us -> 3.76 us
where the time goes in v3:
time: 111 us
  Pallas kernels  106 us (95%)
  local copies, waits for them, and re-layouts  3.76 us (3%)
    pallas_call x1, Pallas kernels, on_device(): pl.pallas_call(layer_kernel, out_shape=(jax.ShapeDtypeStruct((unit, width...  106 us
    unnamed x2, local copies, waits for them, and re-layouts  3.76 us

profile of v3, /device:TPU:2, one launch (start us, length us, event | category | flops | bytes accessed | tf_op | source)
XLA Modules:
  0.0 111.1 jit_solution(8494416129469038736)
XLA Ops:
  0.7 0.8 fusion
  1.5 105.9 %layer.1 = (bf16[128,2048]{1,0:T(8,128)(2,1)}, bf16[128,2048]{1,0:T(8,128)(2,1)}) custom-call(bf16[128,2048]{1,0:T(8,128)(2,1)} %x_ref.1, f32[1,2048]{1,0:T(1,128)} %bitcast.18, s32[1,256]{1,0:T(1,128)} %bitcast.21, f32[2,128]{1,0:T(2,128)} %bitcast.22, bf16[2048,256]{1,0:T(8,128)(2,1)} %bitcast.15, bf16[2048,256]{1,0:T(8,128)(2,1)} %bitcast.16, ...), custom_call_target="tpu_custom_call" | custom-call | tf_op jit(solution)/shard_map/layer/pallas_call | solution.py:699
  107.4 1.9 %copy.20 = bf16[128,2048]{1,0:T(8,128)(2,1)} copy(bf16[128,2048]{1,0:T(8,128)(2,1)} %get-tuple-element.8) | data formatting | bytes 1048576
  109.3 1.9 %copy.21 = bf16[128,2048]{1,0:T(8,128)(2,1)} copy(bf16[128,2048]{1,0:T(8,128)(2,1)} %get-tuple-element.9) | data formatting | bytes 1048576
  (2 shorter events, 0.0 us)

commit v4 on v3

--- a/solution.py
+++ b/solution.py
@@ -2,6 +2,7 @@
 
 import jax
 import jax.numpy as jnp
+import numpy as np
 from jax import lax
 from jax.experimental import pallas as pl
 from jax.experimental.pallas import tpu as pltpu
@@ -16,6 +17,11 @@
 CHUNKS = (1, 1, 1, 1, 1, 1)
 HEAD = 128
 FINE = 64
+TURN = 6.283185307179586
+TURN_HIGH = 6.28125
+TURN_MIDDLE = 2029.0 / 2.0**20
+TURN_LOW = TURN - TURN_HIGH - TURN_MIDDLE
+SETTLE = 2
 MESH_ID = pl.DeviceIdType.MESH
 VMEM_LIMIT = 66060288
 
@@ -184,26 +190,36 @@
 
 
 def layer_kernel(
+    x_hbm,
+    gain_hbm,
+    routes_hbm,
+    score_hbm,
+    gate_hbm,
+    up_hbm,
+    down_hbm,
+    mx_hbm,
+    mx_gain_hbm,
+    q_hbm,
+    k_hbm,
+    v_hbm,
+    g_hbm,
+    head_gain_hbm,
+    o_hbm,
+    log_rows_hbm,
+    rate_hbm,
+    mixed_ref,
+    out_ref,
     x_ref,
     gain_ref,
     routes_ref,
     score_ref,
-    gate_hbm,
-    up_hbm,
-    down_hbm,
-    mx_hbm,
     mx_gain,
-    q_hbm,
-    k_hbm,
-    v_hbm,
-    g_hbm,
     head_gain,
-    o_hbm,
     log_rows_ref,
+    rate_ref,
     cos_ref,
     sin_ref,
-    mixed_ref,
-    out_ref,
+    small_sem,
     picked,
     send_buf,
     arrived,
@@ -266,10 +282,24 @@
     weight_peer = {"tp": (1 - c) * flip + c * mirror}
     token_peer = {"tp": (1 - c) * mirror + c * flip}
     experts = nz * nx * nc
-    tokens, width = x_ref.shape
+    tokens, width = x_hbm.shape
     group = min(32, experts)
     group_count = experts // group
 
+    smalls = []
+    for n, (source, kept) in enumerate(
+        (
+            (x_hbm, x_ref),
+            (gain_hbm, gain_ref),
+            (routes_hbm, routes_ref),
+            (score_hbm, score_ref),
+            (mx_gain_hbm, mx_gain),
+            (head_gain_hbm, head_gain),
+            (log_rows_hbm, log_rows_ref),
+            (rate_hbm, rate_ref),
+        )
+    ):
+        smalls.append(pltpu.make_async_copy(source, kept, small_sem.at[n]))
     slab = nx * nc
     spot = x * nc + c
     loads = [pltpu.make_async_copy(mx_hbm, mx_buf, load_sem.at[0])]
@@ -283,6 +313,8 @@
     ):
         locals_.append(pltpu.make_async_copy(source, target.at[0], weight_local.at[k]))
 
+    for load in smalls:
+        load.start()
     barrier = pltpu.get_barrier_semaphore()
     for_each_peer(
         lambda device, index: pl.semaphore_signal(
@@ -294,6 +326,16 @@
     for load in loads + locals_:
         load.start()
 
+    pl.semaphore_wait(barrier, experts + 1)
+    weights_out = [
+        remote(gate_hbm, gate_buf.at[1], weight_send.at[0], weight_recv.at[0], weight_peer),
+        remote(up_hbm, up_buf.at[1], weight_send.at[1], weight_recv.at[1], weight_peer),
+        remote(down_hbm, down_buf.at[1], weight_send.at[2], weight_recv.at[2], weight_peer),
+    ]
+    for copy in weights_out:
+        copy.start()
+    for load in smalls[:4]:
+        load.wait()
     floats = x_ref[...].astype(jnp.float32)
     scale = lax.rsqrt(jnp.mean(floats * floats, axis=-1, keepdims=True) + EPS)
     normed = (floats * scale * gain_ref[...]).astype(jnp.bfloat16)
@@ -382,19 +424,21 @@
     for p in chunks:
         fold(p, picked, firsts[p] * experts, send_buf)
 
-    pl.semaphore_wait(barrier, experts + 1)
-    weights_out = [
-        remote(gate_hbm, gate_buf.at[1], weight_send.at[0], weight_recv.at[0], weight_peer),
-        remote(up_hbm, up_buf.at[1], weight_send.at[1], weight_recv.at[1], weight_peer),
-        remote(down_hbm, down_buf.at[1], weight_send.at[2], weight_recv.at[2], weight_peer),
-    ]
-    for copy in weights_out:
-        copy.start()
     for p in chunks:
         exchange(p, send_buf, arrived, dispatch_send, dispatch_recv)
 
-    for load in loads:
+    for load in smalls[4:] + loads:
         load.wait()
+    table = cos_ref.shape
+    line = lax.broadcasted_iota(jnp.int32, table, 0)
+    position = jnp.where(line < FINE, line, me * mx_buf.shape[0] + (line - FINE) * FINE)
+    angles = position.astype(jnp.float32) * rate_ref[...]
+    turns = jnp.floor(angles * (1.0 / TURN) + 0.5)
+    angles = ((angles - turns * TURN_HIGH) - turns * TURN_MIDDLE) - turns * TURN_LOW
+    cos_ref[...] = jnp.cos(angles)
+    sin_ref[...] = jnp.where(
+        lax.broadcasted_iota(jnp.int32, table, 1) < HEAD // 2, -1.0, 1.0
+    ) * jnp.sin(angles)
     project_rows(mx_buf, mx_gain, mixer_weights, cos_ref, sin_ref, q_buf, k_buf, v_buf, g_buf)
     scan_blocks(log_rows_ref, q_buf, k_buf, v_buf, inner_buf, update_buf, decay_buf)
     block_count, heads = update_buf.shape[:2]
@@ -646,6 +690,25 @@
     wait_bytes(state_send.at[pl.ds(0, slab - 1)], state_sems.at[0])
     wait_bytes(slab_got.at[pl.ds(0, nz - 1)], state_sems.at[2])
     wait_bytes(enter_send.at[pl.ds(0, slab - 1)], state_sems.at[4])
+
+
+def settle_kernel(mixed, routed, mixed_out, routed_out, mixed_buf, routed_buf, load_sem, store_sem):
+    loads, stores = [], []
+    for n, (source, kept, target) in enumerate(
+        ((mixed, mixed_buf, mixed_out), (routed, routed_buf, routed_out))
+    ):
+        step = source.shape[0] // SETTLE
+        for k in range(SETTLE):
+            part = pl.ds(k * step, step)
+            loads.append(pltpu.make_async_copy(source.at[part], kept.at[part], load_sem.at[n, k]))
+            stores.append(pltpu.make_async_copy(kept.at[part], target.at[part], store_sem.at[n, k]))
+    for load in loads:
+        load.start()
+    for load, store in zip(loads, stores):
+        load.wait()
+        store.start()
+    for store in stores:
+        store.wait()
 
 
 def on_device(
@@ -682,34 +745,34 @@
     bf16, f32 = jnp.bfloat16, jnp.float32
 
     half_dim = HEAD // 2
-    lane = jnp.arange(HEAD, dtype=jnp.int32)
-    frequency = 10000.0 ** (-(lane % half_dim).astype(f32) / half_dim)
-    row = jnp.arange(FINE + mix_rows // FINE, dtype=jnp.int32)
-    coarse = lax.axis_index(EP) * mix_rows + (row - FINE) * FINE
-    position = jnp.where(row < FINE, row, coarse)
-    angles = position.astype(f32)[:, None] * frequency[None, :]
-    cosine = jnp.cos(angles)
-    sine = jnp.where(lane < half_dim, -1.0, 1.0) * jnp.sin(angles)
+    rates = 10000.0 ** (-(np.arange(HEAD) % half_dim) / half_dim)
+    rates = jnp.asarray(rates.reshape(1, HEAD).astype(np.float32))
     log_rows = log_decay.T.reshape(heads, block_count, BLOCK).transpose(1, 0, 2)
 
     vmem = pl.BlockSpec(memory_space=pltpu.VMEM)
-    anywhere = pl.BlockSpec(memory_space=pltpu.HBM)
+    anywhere = pl.BlockSpec(memory_space=pl.ANY)
     dma = pltpu.SemaphoreType.DMA
     chunk_sems = dma((len(CHUNKS),))
-    return pl.pallas_call(
+    mixed, routed = pl.pallas_call(
         layer_kernel,
         out_shape=(
             jax.ShapeDtypeStruct((unit, width), bf16),
             jax.ShapeDtypeStruct((tokens, width), bf16),
         ),
-        in_specs=[vmem] * 4
-        + [anywhere] * 4
-        + [vmem]
-        + [anywhere] * 4
-        + [vmem, anywhere]
-        + [vmem] * 3,
+        in_specs=[anywhere] * 17,
         out_specs=(vmem, vmem),
         scratch_shapes=[
+            pltpu.VMEM((tokens, width), bf16),
+            pltpu.VMEM((1, width), f32),
+            pltpu.VMEM((1, 2 * tokens), jnp.int32),
+            pltpu.VMEM((2, tokens), f32),
+            pltpu.VMEM((1, width), f32),
+            pltpu.VMEM((1, mix_width), f32),
+            pltpu.VMEM((block_count, heads, BLOCK), f32),
+            pltpu.VMEM((1, HEAD), f32),
+            pltpu.VMEM((FINE + mix_rows // FINE, HEAD), f32),
+            pltpu.VMEM((FINE + mix_rows // FINE, HEAD), f32),
+            dma((8,)),
             pltpu.VMEM((CAP * experts, width), bf16),
             messages,
             messages,
@@ -774,9 +837,24 @@
         head_gain.reshape(1, mix_width),
         output_weight,
         log_rows,
-        cosine,
-        sine,
-    )
+        rates,
+    )
+    return pl.pallas_call(
+        settle_kernel,
+        out_shape=(
+            jax.ShapeDtypeStruct(mixed.shape, bf16),
+            jax.ShapeDtypeStruct(routed.shape, bf16),
+        ),
+        in_specs=[anywhere] * 2,
+        out_specs=(anywhere, anywhere),
+        scratch_shapes=[
+            pltpu.VMEM(mixed.shape, bf16),
+            pltpu.VMEM(routed.shape, bf16),
+            dma((2, SETTLE)),
+            dma((2, SETTLE)),
+        ],
+        name="settle",
+    )(mixed, routed)
 
 
 def solution(mesh):

time: 111 us -> 108 us (0.973)
  local copies, waits for them, and re-layouts: 3.76 us -> 0 us
    unnamed x2 -> x0, local copies, waits for them, and re-layouts: 3.76 us -> none
    pallas_call x0 -> x1, Pallas kernels: none -> 1.98 us  [on_device(): pl.pallas_call(settle_kernel, out_shape=(jax.ShapeDtypeStruct(mixed.shape...]
where the time goes in v4:
time: 108 us
  Pallas kernels  107 us (99%)
    pallas_call x1, Pallas kernels, on_device(): pl.pallas_call(layer_kernel, out_shape=(jax.ShapeDtypeStruct((unit, width...  105 us

profile of v4, /device:TPU:2, one launch (start us, length us, event | category | flops | bytes accessed | tf_op | source)
XLA Modules:
  0.0 107.9 jit_solution(9087850521947394992)
XLA Ops:
  0.6 105.1 %layer.1 = (bf16[128,2048]{1,0:T(8,128)(2,1)}, bf16[128,2048]{1,0:T(8,128)(2,1)}) custom-call(bf16[128,2048]{1,0:T(8,128)(2,1)} %x_hbm.1, f32[1,2048]{1,0:T(1,128)} %bitcast.18, s32[1,256]{1,0:T(1,128)} %bitcast.21, f32[2,128]{1,0:T(2,128)} %bitcast.22, bf16[2048,256]{1,0:T(8,128)(2,1)} %bitcast.15, bf16[2048,256]{1,0:T(8,128)(2,1)} %bitcast.16, ...), custom_call_target="tpu_custom_call" | custom-call | tf_op jit(solution)/shard_map/layer/pallas_call | solution.py:756
  105.8 2.0 %settle.1 = (bf16[128,2048]{1,0:T(8,128)(2,1)}, bf16[128,2048]{1,0:T(8,128)(2,1)}) custom-call(bf16[128,2048]{1,0:T(8,128)(2,1)} %get-tuple-element.4.mixed, bf16[128,2048]{1,0:T(8,128)(2,1)} %get-tuple-element.5.routed), custom_call_target="tpu_custom_call" | custom-call | tf_op jit(solution)/shard_map/settle/pallas_call | solution.py:842

commit v5 on v4

--- a/solution.py
+++ b/solution.py
@@ -500,7 +500,7 @@
     def contract(hidden):
         return dot(hidden, down_buf[...].reshape(-1, width))
 
-    def compute(p):
+    def expand(p):
         forwards[p].wait_recv()
         unpack(1, p, passed)
         own_rows = CHUNKS[p] * experts
@@ -512,7 +512,11 @@
             halves.append(
                 (gate_part / (1.0 + jnp.exp(-gate_part)) * up_part).astype(jnp.bfloat16)
             )
-        hidden = jnp.concatenate(halves, axis=1)
+        hiddens[p] = jnp.concatenate(halves, axis=1)
+
+    def project(p):
+        own_rows = CHUNKS[p] * experts
+        hidden = hiddens[p]
         part_send[p][...] = contract(hidden[own_rows:]).astype(jnp.bfloat16)
         parts[p] = remote(
             part_send[p], part_recv[p], part_send_sem.at[p], part_recv_sem.at[p], token_peer
@@ -576,9 +580,11 @@
     for k in range(2):
         locals_[k].wait()
         weights_out[k].wait_recv()
+    expand(0)
+    expand(1)
     locals_[2].wait()
     weights_out[2].wait_recv()
-    compute(0)
+    project(0)
     forward(2)
     wait_bytes(slab_got.at[pl.ds(0, nz - 1)], state_sems.at[3])
     for h in range(heads):
@@ -597,10 +603,11 @@
         ).start()
     )
     enter_got[spot] = enter_send[spot]
-    compute(1)
+    project(1)
     give_back(0)
     forward(3)
-    compute(2)
+    expand(2)
+    project(2)
     wait_bytes(enter_send.at[pl.ds(0, slab - 1)], state_sems.at[5])
     entering = [
         jnp.concatenate([enter_got[n, h] for n in range(slab)], axis=0) for h in range(heads)
@@ -610,12 +617,15 @@
     finish_blocks(
         entering, q_buf, g_buf, inner_buf, update_buf, decay_buf, head_gain, o_buf, mix_buf
     )
-    compute(3)
+    expand(3)
+    project(3)
     give_back(2)
     forward(5)
-    compute(4)
+    expand(4)
+    project(4)
     give_back(3)
-    compute(5)
+    expand(5)
+    project(5)
     unit = mix_buf.shape[0] // 4
     half = width // 2
     right, left = lax.rem(y + 1, 4), lax.rem(y + 3, 4)
@@ -669,6 +679,8 @@
     combine(1)
     combine(2)
     combine(3)
+    combine(4)
+    combine(5)
     for n in range(2):
         directs[2 * n + 1].wait_recv()
         summed[n].wait_recv()
@@ -678,8 +690,6 @@
         + side_got[1].astype(jnp.float32)
     ).astype(jnp.bfloat16)
 
-    combine(4)
-    combine(5)
     for copy in (
         weights_out + list(forwards.values()) + list(parts.values()) + directs + summed
     ):

time: 108 us -> 106 us (0.981)
  Pallas kernels: 107 us -> 105 us
    pallas_call x1, Pallas kernels: 105 us -> 103 us  [on_device(): pl.pallas_call(layer_kernel, out_shape=(jax.ShapeDtypeStruct((unit, width...]
where the time goes in v5:
time: 106 us
  Pallas kernels  105 us (99%)
    pallas_call x1, Pallas kernels, on_device(): pl.pallas_call(layer_kernel, out_shape=(jax.ShapeDtypeStruct((unit, width...  103 us

profile of v5, /device:TPU:2, one launch (start us, length us, event | category | flops | bytes accessed | tf_op | source)
XLA Modules:
  0.0 106.1 jit_solution(7059607565171337078)
XLA Ops:
  0.6 103.3 %layer.1 = (bf16[128,2048]{1,0:T(8,128)(2,1)}, bf16[128,2048]{1,0:T(8,128)(2,1)}) custom-call(bf16[128,2048]{1,0:T(8,128)(2,1)} %x_hbm.1, f32[1,2048]{1,0:T(1,128)} %bitcast.18, s32[1,256]{1,0:T(1,128)} %bitcast.21, f32[2,128]{1,0:T(2,128)} %bitcast.22, bf16[2048,256]{1,0:T(8,128)(2,1)} %bitcast.15, bf16[2048,256]{1,0:T(8,128)(2,1)} %bitcast.16, ...), custom_call_target="tpu_custom_call" | custom-call | tf_op jit(solution)/shard_map/layer/pallas_call | solution.py:766
  103.9 2.0 %settle.1 = (bf16[128,2048]{1,0:T(8,128)(2,1)}, bf16[128,2048]{1,0:T(8,128)(2,1)}) custom-call(bf16[128,2048]{1,0:T(8,128)(2,1)} %get-tuple-element.4.mixed, bf16[128,2048]{1,0:T(8,128)(2,1)} %get-tuple-element.5.routed), custom_call_target="tpu_custom_call" | custom-call | tf_op jit(solution)/shard_map/settle/pallas_call | solution.py:852
